TPU v7x, 32 devices: a whole 2x2x4 slice. The times are simulated.
32 devices in a mesh: sp: 8 (over z, core), tp: 4 (over y, x).
Axes of the slice: x: 2, y: 2, z: 4, core: 2. Of those that a mesh axis runs over, the one named last changes fastest.
Arguments:
- mix_values: bfloat16 [1024, 4096], P('sp', 'tp'), may hold values from -6 to 6
- mix_gate: bfloat16 [1024, 4096], P('sp', 'tp'), may hold values from -6 to 6
- input_keys: bfloat16 [1024, 2048], P('sp', 'tp'), may hold values from -0.31640625 to 0.31640625
- output_keys: bfloat16 [1024, 2048], P('sp', 'tp'), may hold values from -0.31640625 to 0.31640625
- step_sizes: float32 [1024, 64], P('sp', 'tp'), may hold values from 0.1 to 8
- decay_rates: float32 [64], P('tp'), may hold values from 4.8828125e-05 to 0.03
- out_proj: bfloat16 [2048, 4096], P('sp', 'tp'), may hold values from -0.09375 to 0.09375
- expert_inputs: bfloat16 [1024, 2048], P('sp'), may hold values from -20 to 20
- stream_grad: bfloat16 [1024, 2048], P('sp'), may hold values from -6 to 6
- routes: int32 [1024, 2], P('sp'), may hold values from 0 to 7, all different within a row; in each aligned block of 128 rows (0 to 127, 128 to 255, ...) at most 48 rows name the same one
- route_weights: float32 [1024, 2], P('sp'), may hold values from 0.1 to 0.9
- gate_proj: bfloat16 [8, 2048, 2048], P('sp', 'tp'), may hold values from -0.125 to 0.125
- up_proj: bfloat16 [8, 2048, 2048], P('sp', 'tp'), may hold values from -0.125 to 0.125
- down_proj: bfloat16 [8, 2048, 2048], P('sp', 'tp'), may hold values from -0.125 to 0.125
Outputs:
- grad_gate_proj: bfloat16 [8, 2048, 2048], P('sp', 'tp')
- grad_up_proj: bfloat16 [8, 2048, 2048], P('sp', 'tp')
- grad_down_proj: bfloat16 [8, 2048, 2048], P('sp', 'tp')
- grad_out_proj: float32 [2048, 4096], P('sp', 'tp')
- grad_values: bfloat16 [1024, 4096], P('sp', 'tp')
- grad_gate: bfloat16 [1024, 4096], P('sp', 'tp')
- grad_input_keys: bfloat16 [1024, 2048], P('sp', 'tp')
- grad_output_keys: bfloat16 [1024, 2048], P('sp', 'tp')
- grad_steps: float32 [1024, 64], P('sp', 'tp')
Inputs may be any that keep to these rules, and one draw needn't show every extreme that they name: In the rows of one device no expert is named by more than 48 routes, and on some devices one expert is named by exactly 48; the 2 routes of a token name different experts.
All inputs are finite; a program needn't handle non-finite values.
Results may differ from a plain program's by a relative error of at most 0.025.
Values may be sent and summed in bfloat16 or wider, within the bound.
A program may use at most 64 MiB of HBM per device.

v0:
```python
import functools

import jax
import jax.numpy as jnp
from jax import lax
from jax.experimental import pallas as pl
from jax.experimental.pallas import tpu as pltpu
from jax.sharding import PartitionSpec as P

NSTATE = 128
TAIL = 16
TERMS = 3
CLAMP_LIMIT = 7.0
SIGMOID_SCALE = 1.702
HIGHEST = lax.Precision.HIGHEST
F32 = jnp.float32
BF16 = jnp.bfloat16
NN = (((1,), (0,)), ((), ()))
NT = (((1,), (1,)), ((), ()))
TN = (((0,), (0,)), ((), ()))


def mm(a, b, dims=NN):
    return lax.dot_general(a, b, dims, preferred_element_type=F32)


def mm_exact(a, b, dims=NN):
    return lax.dot_general(a, b, dims, precision=HIGHEST, preferred_element_type=F32)


def grid_of(rows, cols):
    return (
        lax.broadcasted_iota(jnp.int32, (rows, cols), 0),
        lax.broadcasted_iota(jnp.int32, (rows, cols), 1),
    )


def spread(heads, size):
    at, col = grid_of(heads, heads * size)
    return ((col >= at * size) & (col < (at + 1) * size)).astype(F32)


def fold(heads, size):
    col, at = grid_of(heads * size, heads)
    return ((col >= at * size) & (col < (at + 1) * size)).astype(F32)


def call(kernel, outs, flops, *args, vmem=None):
    bytes_accessed = sum(a.size * a.dtype.itemsize for a in args)
    bytes_accessed += sum(o.size * o.dtype.itemsize for o in outs)
    return pl.pallas_call(
        kernel,
        out_shape=outs,
        in_specs=[pl.BlockSpec(memory_space=pltpu.VMEM)] * len(args),
        out_specs=[pl.BlockSpec(memory_space=pltpu.VMEM)] * len(outs),
        cost_estimate=pl.CostEstimate(
            flops=flops, bytes_accessed=bytes_accessed, transcendentals=0
        ),
        compiler_params=pltpu.CompilerParams(vmem_limit_bytes=vmem or 24 * 2**20),
    )(*args)


def out(shape, dtype):
    return jax.ShapeDtypeStruct(shape, dtype)


def dispatch_kernel(experts, cap, width, routes_ref, weights_ref, x_ref, g_ref, xs_ref, gs_ref, sel_ref):
    tokens, top = routes_ref.shape
    start = pl.multiple_of(lax.axis_index("tp") * width, 128)
    x = x_ref[:, pl.ds(start, width)]
    g = g_ref[:, pl.ds(start, width)].astype(F32)
    _, expert = grid_of(tokens, experts)
    _, slot = grid_of(tokens, experts * cap)
    row, col = grid_of(tokens, tokens)
    hits = [expert == routes_ref[:, k : k + 1] for k in range(top)]
    named = sum(hit.astype(F32) for hit in hits)
    before = mm((row > col).astype(BF16), named.astype(BF16))
    every = jnp.zeros((tokens, experts * cap), F32)
    grads = jnp.zeros((experts * cap, width), F32)
    for k in range(top):
        rank = jnp.sum(jnp.where(hits[k], before, 0.0), axis=1, keepdims=True).astype(jnp.int32)
        chosen = (slot == routes_ref[:, k : k + 1] * cap + rank).astype(F32)
        every = every + chosen
        grads = grads + mm(chosen.astype(BF16), (g * weights_ref[:, k : k + 1]).astype(BF16), TN)
    picked = every.astype(BF16)
    sel_ref[...] = picked
    xs_ref[...] = mm(picked, x, TN).astype(BF16)
    gs_ref[...] = grads.astype(BF16)


def combine_kernel(width, sel_ref, back_ref, g_ref, out_ref):
    start = pl.multiple_of(lax.axis_index("tp") * width, 128)
    g = g_ref[:, pl.ds(start, width)].astype(F32)
    out_ref[...] = (g + mm(sel_ref[...], back_ref[...])).astype(BF16)


def mixing_of(log_ref, logt_ref, h):
    length = log_ref.shape[0]
    row, col = grid_of(length, length)
    gap = log_ref[:, h : h + 1] - logt_ref[h : h + 1, :]
    return jnp.where(row >= col, jnp.exp(jnp.minimum(gap, 0.0)), 0.0)


def local_kernel(groups, v_ref, b_ref, c_ref, steps_ref, log_ref, logt_ref, y_ref, state_ref):
    heads = steps_ref.shape[1]
    per, size = heads // groups, v_ref.shape[1] // heads
    wide = per * size
    length = v_ref.shape[0]
    expand = spread(heads, size)
    to_end = jnp.exp(log_ref[length - 1 :, :] - log_ref[...])
    x = v_ref[...].astype(F32) * mm_exact(steps_ref[...], expand)
    xe = (x * mm_exact(to_end, expand)).astype(BF16)
    x = x.astype(BF16)
    for g in range(groups):
        keys = b_ref[:, g * NSTATE : (g + 1) * NSTATE]
        scores = mm(c_ref[:, g * NSTATE : (g + 1) * NSTATE], keys, NT)
        parts = []
        for r in range(per):
            h = g * per + r
            att = (scores * mixing_of(log_ref, logt_ref, h)).astype(BF16)
            parts.append(mm(att, x[:, h * size : (h + 1) * size]))
        y_ref[:, g * wide : (g + 1) * wide] = jnp.concatenate(parts, axis=1)
        state_ref[g * wide : (g + 1) * wide, :] = mm(
            xe[:, g * wide : (g + 1) * wide], keys, TN
        ).astype(BF16)
    at, lane = grid_of(heads, NSTATE)
    rest = mm_exact(log_ref[length - 1 :, :], (at == lane).astype(F32))
    row, _ = grid_of(TAIL, NSTATE)
    tail = jnp.zeros((TAIL, NSTATE), F32)
    for k in range(TERMS):
        term = rest.astype(BF16).astype(F32)
        tail = jnp.where(row == k, term, tail)
        rest = rest - term
    state_ref[groups * wide :, :] = tail.astype(BF16)


def weighted_state(all_ref, weights_ref, g, r, per, size):
    h = g * per + r
    total = jnp.zeros((size, NSTATE), F32)
    for j in range(all_ref.shape[0]):
        part = all_ref[j, h * size : (h + 1) * size, :].astype(F32)
        total = total + weights_ref[j : j + 1, h : h + 1] * part
    return total


def enter_kernel(groups, all_ref, weights_ref, y_ref, gate_ref, c_ref, log_ref, out_ref, gated_ref, state_ref):
    heads = log_ref.shape[1]
    per, size = heads // groups, y_ref.shape[1] // heads
    wide = per * size
    decay = mm_exact(jnp.exp(log_ref[...]), spread(heads, size))
    for g in range(groups):
        state = jnp.concatenate(
            [weighted_state(all_ref, weights_ref, g, r, per, size) for r in range(per)], axis=0
        ).astype(BF16)
        state_ref[g] = state
        at = slice(g * wide, (g + 1) * wide)
        entered = mm(c_ref[:, g * NSTATE : (g + 1) * NSTATE], state, NT) * decay[:, at]
        mixed = y_ref[:, at] + entered
        out_ref[:, at] = mixed
        gate = gate_ref[:, at].astype(F32)
        gated_ref[:, at] = (mixed * gate * jax.nn.sigmoid(gate)).astype(BF16)


def gate_kernel(groups, grad_ref, out_ref, gate_ref, c_ref, log_ref, gate_grad_ref, mixer_ref, state_ref):
    heads = log_ref.shape[1]
    wide = grad_ref.shape[1] // groups
    decay = mm_exact(jnp.exp(log_ref[...]), spread(heads, grad_ref.shape[1] // heads))
    for g in range(groups):
        at = slice(g * wide, (g + 1) * wide)
        gate = gate_ref[:, at].astype(F32)
        sig = jax.nn.sigmoid(gate)
        grad = grad_ref[:, at]
        gate_grad_ref[:, at] = (grad * out_ref[:, at] * sig * (1.0 + gate * (1.0 - sig))).astype(BF16)
        mixer = grad * gate * sig
        mixer_ref[:, at] = mixer
        keys = c_ref[:, g * NSTATE : (g + 1) * NSTATE]
        state_ref[at, :] = mm((mixer * decay[:, at]).astype(BF16), keys, TN).astype(BF16)


def inner_kernel(
    groups, v_ref, b_ref, c_ref, steps_ref, log_ref, logt_ref, mixer_ref, state_ref,
    out_keys_ref, in_part_ref, x_part_ref, base_ref,
):
    heads = steps_ref.shape[1]
    per, size = heads // groups, v_ref.shape[1] // heads
    wide = per * size
    length = v_ref.shape[0]
    row, col = grid_of(length, length)
    later = (row <= col).astype(BF16)
    expand = spread(heads, size)
    mixer = mixer_ref[...]
    decayed = mixer * mm_exact(jnp.exp(log_ref[...]), expand)
    decayed_low = decayed.astype(BF16)
    mixer = mixer.astype(BF16)
    x = (v_ref[...].astype(F32) * mm_exact(steps_ref[...], expand)).astype(BF16)
    entering = []
    _, head_at = grid_of(length, heads)
    pairs = jnp.zeros((length, heads), F32)
    for g in range(groups):
        at = slice(g * wide, (g + 1) * wide)
        keys_in = b_ref[:, g * NSTATE : (g + 1) * NSTATE]
        keys_out = c_ref[:, g * NSTATE : (g + 1) * NSTATE]
        scores = mm(keys_out, keys_in, NT)
        score_grad = jnp.zeros((length, length), F32)
        parts = []
        for r in range(per):
            h = g * per + r
            here = slice(h * size, (h + 1) * size)
            mixing = mixing_of(log_ref, logt_ref, h)
            att = scores * mixing
            att_grad = mm(mixer[:, here], x[:, here], NT)
            parts.append(mm(att.astype(BF16), mixer[:, here], TN))
            score_grad = score_grad + att_grad * mixing
            after = mm(later, (att_grad * att).astype(BF16))
            crossing = jnp.sum(jnp.where(col < row, after, 0.0), axis=1, keepdims=True)
            pairs = pairs + jnp.where(head_at == h, crossing, 0.0)
        x_part_ref[:, at] = jnp.concatenate(parts, axis=1)
        score_grad = score_grad.astype(BF16)
        state = state_ref[g]
        out_keys_ref[:, g * NSTATE : (g + 1) * NSTATE] = (
            mm(score_grad, keys_in) + mm(decayed_low[:, at], state)
        ).astype(BF16)
        in_part_ref[:, g * NSTATE : (g + 1) * NSTATE] = mm(score_grad, keys_out, TN)
        entering.append(decayed[:, at] * mm(keys_out, state, NT))
    entering = jnp.concatenate(entering, axis=1)
    sums = mm_exact(entering, fold(heads, size))
    base_ref[...] = pairs + mm_exact((row <= col).astype(F32), sums)


def outer_kernel(
    groups, all_ref, weights_ref, state_ref, v_ref, b_ref, steps_ref, log_ref, rates_ref,
    in_part_ref, x_part_ref, base_ref, values_ref, in_keys_ref, steps_grad_ref,
):
    heads = steps_ref.shape[1]
    per, size = heads // groups, v_ref.shape[1] // heads
    wide = per * size
    length = v_ref.shape[0]
    row, col = grid_of(length, length)
    expand = spread(heads, size)
    last = log_ref[length - 1 :, :]
    steps = mm_exact(steps_ref[...], expand)
    to_end = mm_exact(jnp.exp(last - log_ref[...]), expand)
    values = v_ref[...].astype(F32)
    xe = values * steps * to_end
    xe_low = xe.astype(BF16)
    leaving, direct = [], []
    _, head_at = grid_of(1, heads)
    passing = jnp.zeros((1, heads), F32)
    for g in range(groups):
        at = slice(g * wide, (g + 1) * wide)
        keys_in = b_ref[:, g * NSTATE : (g + 1) * NSTATE]
        tiles = [weighted_state(all_ref, weights_ref, g, r, per, size) for r in range(per)]
        for r in range(per):
            before = state_ref[g, r * size : (r + 1) * size, :].astype(F32)
            both = jnp.sum(jnp.sum(tiles[r] * before, axis=0, keepdims=True), axis=1, keepdims=True)
            passing = passing + jnp.where(head_at == g * per + r, both, 0.0)
        after = jnp.concatenate(tiles, axis=0).astype(BF16)
        reached = mm(keys_in, after, NT)
        x_grad = x_part_ref[:, at] + reached * to_end[:, at]
        values_ref[:, at] = (x_grad * steps[:, at]).astype(BF16)
        in_keys_ref[:, g * NSTATE : (g + 1) * NSTATE] = (
            in_part_ref[:, g * NSTATE : (g + 1) * NSTATE] + mm(xe_low[:, at], after)
        ).astype(BF16)
        leaving.append(reached * xe[:, at])
        direct.append(x_grad * values[:, at])
    gather = fold(heads, size)
    leaving = mm_exact(jnp.concatenate(leaving, axis=1), gather)
    direct = mm_exact(jnp.concatenate(direct, axis=1), gather)
    crossing = base_ref[...] + mm_exact((col < row).astype(F32), leaving) + jnp.exp(last) * passing
    steps_grad_ref[...] = direct - rates_ref[...] * crossing


def side_by_side(stacked):
    return jnp.concatenate([stacked[c] for c in range(stacked.shape[0])], axis=-1)


def body(
    mix_values,
    mix_gate,
    input_keys,
    output_keys,
    step_sizes,
    decay_rates,
    out_proj,
    expert_inputs,
    stream_grad,
    routes,
    route_weights,
    gate_proj,
    up_proj,
    down_proj,
):
    tok_rows = mix_values.shape[0]
    model_width = stream_grad.shape[1]
    top = routes.shape[1]
    sp_devices = lax.axis_size("sp")
    tp_devices = lax.axis_size("tp")
    experts = gate_proj.shape[0] * sp_devices
    cap = 3 * tok_rows * top // (2 * experts)
    slots = experts * cap
    heads = step_sizes.shape[1]
    groups = input_keys.shape[1] // NSTATE
    inner = mix_values.shape[1]
    size = inner // heads
    wide = inner // groups
    width = model_width // tp_devices
    state_shape = (groups, wide, NSTATE)
    pair_flops = 2 * tok_rows * tok_rows * inner

    row, col = grid_of(tok_rows, tok_rows)
    rates = decay_rates.reshape(1, heads)
    drop = -step_sizes * rates
    log_decay = mm_exact((row >= col).astype(F32), drop)
    log_decay_t = log_decay.T
    y_local, own_state = call(
        functools.partial(local_kernel, groups),
        [out((tok_rows, inner), F32), out((inner + TAIL, NSTATE), BF16)],
        3 * pair_flops,
        mix_values, input_keys, output_keys, step_sizes, log_decay, log_decay_t,
    )
    all_states = lax.all_gather(own_state, "sp", axis=0)

    send_rows, send_grad, chosen = call(
        functools.partial(dispatch_kernel, experts, cap, width),
        [out((slots, width), BF16), out((slots, width), BF16), out((tok_rows, slots), BF16)],
        6 * tok_rows * slots * width,
        routes, route_weights, expert_inputs, stream_grad,
    )

    def over_sp(rows):
        return lax.all_to_all(
            rows.reshape(experts, cap, width), "sp", split_axis=0, concat_axis=0, tiled=True
        ).reshape(slots, width)

    def over_tp(part):
        copies = jnp.broadcast_to(part[None], (tp_devices,) + part.shape)
        return lax.all_to_all(copies, "tp", split_axis=0, concat_axis=0, tiled=True)

    got_rows = over_sp(send_rows)
    got_grad, all_states = lax.optimization_barrier((over_sp(send_grad), all_states))
    in_rows = side_by_side(over_tp(got_rows))
    grad_rows = side_by_side(over_tp(got_grad))

    spans = jnp.sum(all_states[:, inner : inner + TERMS, :heads].astype(F32), axis=1)
    here = lax.axis_index("sp")
    order = jnp.arange(sp_devices)
    one, two = order[:, None], order[None, :]
    forward = mm_exact(((two > one) & (two < here)).astype(F32), spans)
    forward = jnp.where(one < here, jnp.exp(forward), 0.0)
    backward = mm_exact(((two < one) & (two > here)).astype(F32), spans)
    backward = jnp.where(one > here, jnp.exp(backward), 0.0)
    mixer_out, gated_out, state_in = call(
        functools.partial(enter_kernel, groups),
        [out((tok_rows, inner), F32), out((tok_rows, inner), BF16), out(state_shape, BF16)],
        2 * pair_flops,
        all_states, forward, y_local, mix_gate, output_keys, log_decay,
    )
    gate_weight = gate_proj.reshape(-1, model_width)
    up_weight = up_proj.reshape(-1, model_width)
    down_weight = down_proj.reshape(-1, model_width)
    gate_pre = mm(in_rows, gate_weight, NT)
    up_pre = mm(in_rows, up_weight, NT)
    gate_clamped = jnp.minimum(gate_pre, CLAMP_LIMIT)
    up_clamped = jnp.clip(up_pre, -CLAMP_LIMIT, CLAMP_LIMIT)
    gate_sigmoid = jax.nn.sigmoid(SIGMOID_SCALE * gate_clamped)
    activation = ((up_clamped + 1.0) * gate_clamped * gate_sigmoid).astype(BF16)
    act_grad = mm(grad_rows, down_weight, NT)
    gate_grad = jnp.where(
        gate_pre < CLAMP_LIMIT,
        act_grad
        * (up_clamped + 1.0)
        * gate_sigmoid
        * (1.0 + SIGMOID_SCALE * gate_clamped * (1.0 - gate_sigmoid)),
        0.0,
    ).astype(BF16)
    up_grad = jnp.where(
        jnp.abs(up_pre) < CLAMP_LIMIT, act_grad * gate_clamped * gate_sigmoid, 0.0
    ).astype(BF16)
    back = (mm(gate_grad, gate_weight) + mm(up_grad, up_weight)).astype(BF16)
    grad_down_proj = mm(activation, grad_rows, TN).astype(BF16).reshape(down_proj.shape)
    grad_gate_proj = mm(gate_grad, in_rows, TN).astype(BF16).reshape(gate_proj.shape)
    grad_up_proj = mm(up_grad, in_rows, TN).astype(BF16).reshape(up_proj.shape)

    full_proj = lax.all_gather(out_proj, "sp", axis=0, tiled=True)
    back, full_proj, gated_out = lax.optimization_barrier((back, full_proj, gated_out))
    all_gated = lax.all_gather(gated_out, "sp", axis=0, tiled=True)
    shares = jnp.stack([back[:, c * width : (c + 1) * width] for c in range(tp_devices)])
    shares = lax.all_to_all(shares, "tp", split_axis=0, concat_axis=0, tiled=True)
    reduced = jnp.sum(shares.astype(F32), axis=0).astype(BF16)
    returned = lax.all_to_all(
        reduced.reshape(experts, cap, width), "sp", split_axis=0, concat_axis=0, tiled=True
    ).reshape(slots, width)
    stream_part = call(
        functools.partial(combine_kernel, width),
        [out((tok_rows, width), BF16)],
        2 * tok_rows * slots * width,
        chosen, returned, stream_grad,
    )[0]
    stream_part, all_gated = lax.optimization_barrier((stream_part, all_gated))
    stream_total = lax.all_gather(stream_part, "tp", axis=1, tiled=True)

    gated_grad = mm(stream_total, full_proj)
    grad_gate, mixer_grad, own_grad = call(
        functools.partial(gate_kernel, groups),
        [out((tok_rows, inner), BF16), out((tok_rows, inner), F32), out((inner, NSTATE), BF16)],
        pair_flops,
        gated_grad, mixer_out, mix_gate, output_keys, log_decay,
    )
    all_grads = lax.all_gather(own_grad, "sp", axis=0)
    share = model_width // sp_devices
    all_stream = lax.all_to_all(
        stream_total, "sp", split_axis=1, concat_axis=0, tiled=True
    ).reshape(sp_devices * tok_rows, share)
    grad_out_proj = mm(all_stream, all_gated, TN)
    grad_output_keys, in_part, x_part, base = call(
        functools.partial(inner_kernel, groups),
        [
            out(output_keys.shape, BF16),
            out(input_keys.shape, F32),
            out((tok_rows, inner), F32),
            out((tok_rows, heads), F32),
        ],
        6 * pair_flops,
        mix_values, input_keys, output_keys, step_sizes, log_decay, log_decay_t, mixer_grad, state_in,
    )
    grad_values, grad_input_keys, grad_steps = call(
        functools.partial(outer_kernel, groups),
        [
            out((tok_rows, inner), BF16),
            out(input_keys.shape, BF16),
            out((tok_rows, heads), F32),
        ],
        3 * pair_flops,
        all_grads, backward, state_in, mix_values, input_keys, step_sizes, log_decay, rates,
        in_part, x_part, base,
    )
    return (
        grad_gate_proj,
        grad_up_proj,
        grad_down_proj,
        grad_out_proj,
        grad_values,
        grad_gate,
        grad_input_keys,
        grad_output_keys,
        grad_steps,
    )


def solution(mesh):
    return jax.shard_map(
        body,
        mesh=mesh,
        in_specs=(
            P("sp", "tp"),
            P("sp", "tp"),
            P("sp", "tp"),
            P("sp", "tp"),
            P("sp", "tp"),
            P("tp"),
            P("sp", "tp"),
            P("sp", None),
            P("sp", None),
            P("sp", None),
            P("sp", None),
            P("sp", "tp", None),
            P("sp", "tp", None),
            P("sp", "tp", None),
        ),
        out_specs=(
            P("sp", "tp", None),
            P("sp", "tp", None),
            P("sp", "tp", None),
            P("sp", "tp"),
            P("sp", "tp"),
            P("sp", "tp"),
            P("sp", "tp"),
            P("sp", "tp"),
            P("sp", "tp"),
        ),
        check_vma=False,
    )
```

profile of v0, /device:TPU:1, one launch (start us, length us, event | category | flops | bytes accessed | tf_op | source)
XLA Modules:
  0.0 233.9 jit_solution(17987766359438065075)
XLA Ops:
  7.2 0.9 copy.36.steps_ref
  8.2 0.9 fusion.18
  9.2 0.9 copy-done.1
  10.2 0.9 copy-done.7
  11.1 0.9 copy-done.9
  12.0 2.5 %shard_map.206 = (f32[128,1024]{1,0:T(8,128)S(1)}, bf16[1040,128]{1,0:T(8,128)(2,1)}) custom-call(bf16[128,1024]{1,0:T(8,128)(2,1)S(1)} %copy-done.1, bf16[128,512]{1,0:T(8,128)(2,1)S(1)} %copy-done.9, bf16[128,512]{1,0:T(8,128)(2,1)S(1)} %copy-done.7, f32[128,16]{1,0:T(8,128)S(1)} %copy.36.steps_ref, f32[128,16]{1,0:T(8,128)S(1)} %copy.37.log_ref, ...), custom_call_target="tpu_custom_call" | custom-call | flops 100663296 | bytes 1339392 | tf_op jit(solution)/shard_map/pallas_call | solution.py:51
  17.6 1.0 copy-done.5
  18.6 1.0 copy-done.16
  19.7 1.0 shard_map.205
  20.7 28.7 %all_to_all.49 = bf16[8,48,512]{2,1,0:T(8,128)(2,1)S(1)} all-to-all(bf16[8,48,512]{2,1,0:T(8,128)(2,1)S(1)} %bitcast.77), channel_id=1, replica_groups=mesh['sp'=8,'tp'=4] {'sp'}, dimensions={0} | all-to-all | bytes 786432 | tf_op jit(solution)/shard_map/all_to_all | solution.py:331
  49.4 15.0 %all_to_all.50 = bf16[8,48,512]{2,1,0:T(8,128)(2,1)S(1)} all-to-all(bf16[8,48,512]{2,1,0:T(8,128)(2,1)S(1)} %bitcast.76), channel_id=1, replica_groups=mesh['sp'=8,'tp'=4] {'sp'}, dimensions={0} | all-to-all | bytes 786432 | tf_op jit(solution)/shard_map/all_to_all | solution.py:331
  64.4 1.3 broadcast_in_dim.39
  65.6 4.3 %all-to-all-start.1 = ((bf16[4,384,512]{2,1,0:T(8,128)(2,1)}), bf16[4,384,512]{2,1,0:T(8,128)(2,1)}, u32[]{:S(2)}, u32[]{:S(2)}) async-start(bf16[4,384,512]{2,1,0:T(8,128)(2,1)} %broadcast_in_dim.39), calls=%async_computation.1 | async-start | bytes 3145728 | tf_op jit(solution)/shard_map/all_to_all | solution.py:337
  70.0 18.8 %all-to-all-done.1 = bf16[4,384,512]{2,1,0:T(8,128)(2,1)} async-done(((bf16[4,384,512]{2,1,0:T(8,128)(2,1)}), bf16[4,384,512]{2,1,0:T(8,128)(2,1)}, u32[]{:S(2)}, u32[]{:S(2)}) %all-to-all-start.1) | async-done | bytes 1572896 | tf_op jit(solution)/shard_map/all_to_all | solution.py:337
  88.8 1.3 broadcast_in_dim.40
  90.1 4.4 %all-to-all-start.3 = ((bf16[4,384,512]{2,1,0:T(8,128)(2,1)}), bf16[4,384,512]{2,1,0:T(8,128)(2,1)}, u32[]{:S(2)}, u32[]{:S(2)}) async-start(bf16[4,384,512]{2,1,0:T(8,128)(2,1)} %broadcast_in_dim.40), calls=%async_computation.3 | async-start | bytes 3145728 | tf_op jit(solution)/shard_map/all_to_all | solution.py:337
  94.5 1.5 slice_bitcast_fusion.7
  96.0 1.9 fusion.10
  98.4 1.9 fusion.4
  100.5 1.6 shard_map.207
  102.2 11.1 %all-to-all-done.3 = bf16[4,384,512]{2,1,0:T(8,128)(2,1)} async-done(((bf16[4,384,512]{2,1,0:T(8,128)(2,1)}), bf16[4,384,512]{2,1,0:T(8,128)(2,1)}, u32[]{:S(2)}, u32[]{:S(2)}) %all-to-all-start.3) | async-done | bytes 1572896 | tf_op jit(solution)/shard_map/all_to_all | solution.py:337
  113.3 1.6 slice_bitcast_fusion.3
  115.5 2.6 %select_convert_fusion = (bf16[384,512]{1,0:T(8,128)(2,1)S(1)}, bf16[384,512]{1,0:T(8,128)(2,1)S(1)}) fusion(f32[384,512]{1,0:T(8,128)} %fusion.4, f32[384,512]{1,0:T(8,128)S(1)} %copy-done.47, bf16[1,512,2048]{2,1,0:T(8,128)(2,1)S(1)} %copy-done.46, bf16[384,512]{1,0:T(8,128)(2,1)S(1)} %get-tuple-element.88, bf16[384,512]{1,0:T(8,128)(2,1)S(1)} %get-tuple-element.89, ...), kind=kOutput, calls=%fused_computation.24 | convolution fusion | flops 815923200 | bytes 6029312 | tf_op jit(solution)/shard_map/dot_general | solution.py:24
  118.2 1.0 fusion.8
  119.2 0.9 copy-done.26
  120.1 2.1 add_convert_fusion
  122.3 1.5 slice_bitcast_fusion.11
  123.9 21.3 %all_to_all.51 = bf16[4,384,512]{2,1,0:T(8,128)(2,1)} all-to-all(bf16[4,384,512]{2,1,0:T(8,128)(2,1)S(1)} %pad_maximum_fusion.2), channel_id=1, replica_groups=mesh['sp'=8,'tp'=4] {'tp'}, dimensions={0} | all-to-all | bytes 3145728 | tf_op jit(solution)/shard_map/all_to_all | solution.py:388
  145.2 2.5 %reduce_sum.22 = bf16[384,512]{1,0:T(8,128)(2,1)} reduce(bf16[4,384,512]{2,1,0:T(8,128)(2,1)} %all_to_all.51, bf16[]{:T(256)} %constant.18.clone.1), dimensions={0}, to_apply=%region_1.2 | reduce | flops 589824 | bytes 1966082 | tf_op jit(solution)/shard_map/reduce_sum | solution.py:389
  147.7 17.7 %all_to_all.52 = bf16[8,48,512]{2,1,0:T(8,128)(2,1)S(1)} all-to-all(bf16[8,48,512]{2,1,0:T(8,128)(2,1)} %bitcast.83), channel_id=1, replica_groups=mesh['sp'=8,'tp'=4] {'sp'}, dimensions={0} | all-to-all | bytes 786432 | tf_op jit(solution)/shard_map/all_to_all | solution.py:390
  165.4 0.9 copy-done.23
  166.6 7.4 %all_gather.25 = bf16[128,2048]{1,0:T(8,128)(2,1)S(1)} all-gather(bf16[128,512]{1,0:T(8,128)(2,1)S(1)} %shard_map.208), channel_id=1, replica_groups=mesh['sp'=8,'tp'=4] {'tp'}, dimensions={1}, use_global_device_ids=true | all-gather | bytes 655360 | tf_op jit(solution)/shard_map/all_gather | solution.py:400
  174.0 3.0 %fusion.35.grad_ref = f32[128,1024]{1,0:T(8,128)S(1)} fusion(bf16[128,2048]{1,0:T(8,128)(2,1)S(1)} %all_gather.25, bf16[2048,1024]{1,0:T(8,128)(2,1)} %all-gather.7.cloned.1.call-done), kind=kOutput, calls=%fused_computation.67 | convolution fusion | flops 536870912 | bytes 5242880 | tf_op jit(solution)/shard_map/dot_general | solution.py:24
  177.0 1.3 shard_map.209
  178.3 0.9 copy-done.19
  180.0 0.9 copy.48
  180.9 7.1 %all-to-all-start.6 = ((bf16[128,8,256]{2,0,1:T(8,128)(2,1)}), bf16[128,8,256]{2,0,1:T(8,128)(2,1)}, u32[]{:S(2)}, u32[]{:S(2)}) async-start(bf16[128,8,256]{2,0,1:T(8,128)(2,1)} %bitcast.82), calls=%async_computation.6 | async-start | bytes 1048576 | tf_op jit(solution)/shard_map/all_to_all | solution.py:411
  188.0 4.4 %fusion.1 = bf16[1,512,2048]{2,1,0:T(8,128)(2,1)} fusion(bf16[384,512]{1,0:T(8,128)(2,1)} %copy-done.27, bf16[384,512]{1,0:T(8,128)(2,1)} %copy-done.30, bf16[384,512]{1,0:T(8,128)(2,1)} %copy-done.32, bf16[384,512]{1,0:T(8,128)(2,1)} %copy-done.34, bf16[384,512]{1,0:T(8,128)(2,1)} %copy-done.28), kind=kOutput, calls=%fused_computation.5 | convolution fusion | flops 812646400 | bytes 4063232 | tf_op jit(solution)/shard_map/dot_general | solution.py:24
  192.5 2.6 %fusion = bf16[1,512,2048]{2,1,0:T(8,128)(2,1)} fusion(bf16[384,512]{1,0:T(8,128)(2,1)S(1)} %copy-done.45, bf16[384,512]{1,0:T(8,128)(2,1)S(1)} %copy-done.31, bf16[384,512]{1,0:T(8,128)(2,1)S(1)} %copy-done.33, bf16[384,512]{1,0:T(8,128)(2,1)S(1)} %copy-done.35, bf16[384,512]{1,0:T(8,128)(2,1)S(1)} %copy-done.29), kind=kOutput, calls=%fused_computation.4 | convolution fusion | flops 812646400 | bytes 4063232 | tf_op jit(solution)/shard_map/dot_general | solution.py:24
  195.2 2.7 %fusion.2 = bf16[1,512,2048]{2,1,0:T(8,128)(2,1)} fusion(f32[384,512]{1,0:T(8,128)S(1)} %copy-done.48, f32[384,512]{1,0:T(8,128)S(1)} %copy-done.49, bf16[384,512]{1,0:T(8,128)(2,1)S(1)} %copy-done.39, bf16[384,512]{1,0:T(8,128)(2,1)S(1)} %copy-done.41, bf16[384,512]{1,0:T(8,128)(2,1)S(1)} %copy-done.43, bf16[384,512]{1,0:T(8,128)(2,1)S(1)} %copy-done.37), kind=kOutput, calls=%fused_computation.6 | convolution fusion | flops 814612480 | bytes 5242880 | tf_op jit(solution)/shard_map/dot_general | solution.py:24
  197.9 4.3 %shard_map.210 = (bf16[128,512]{1,0:T(8,128)(2,1)}, f32[128,512]{1,0:T(8,128)S(1)}, f32[128,1024]{1,0:T(8,128)S(1)}, f32[128,16]{1,0:T(8,128)S(1)}) custom-call(bf16[128,1024]{1,0:T(8,128)(2,1)S(1)} %copy-done.2, bf16[128,512]{1,0:T(8,128)(2,1)S(1)} %copy-done.10, bf16[128,512]{1,0:T(8,128)(2,1)S(1)} %copy-done.8, f32[128,16]{1,0:T(8,128)S(1)} %copy.36.steps_ref, ...), custom_call_target="tpu_custom_call" | custom-call | flops 201326592 | bytes 2260992 | tf_op jit(solution)/shard_map/pallas_call | solution.py:51
  202.2 0.8 copy-done.14
  203.0 13.1 %all-to-all-done.6 = bf16[128,8,256]{2,0,1:T(8,128)(2,1)} async-done(((bf16[128,8,256]{2,0,1:T(8,128)(2,1)}), bf16[128,8,256]{2,0,1:T(8,128)(2,1)}, u32[]{:S(2)}, u32[]{:S(2)}) %all-to-all-start.6) | async-done | bytes 524320 | tf_op jit(solution)/shard_map/all_to_all | solution.py:411
  216.2 3.5 %fusion.34 = f32[256,1024]{1,0:T(8,128)} fusion(bf16[1024,256]{1,0:T(8,128)(2,1)} %bitcast.27, bf16[1024,1024]{1,0:T(8,128)(2,1)} %all-gather.9.cloned.1.call-done), kind=kOutput, calls=%fused_computation.66 | convolution fusion | flops 536870912 | bytes 3670016 | tf_op jit(solution)/shard_map/dot_general | solution.py:24
  219.7 1.8 all-gather.13.cloned.1.call-done
  221.4 1.6 copy-done.4
  223.0 1.0 copy-done.15
  224.1 2.6 %shard_map.211 = (bf16[128,1024]{1,0:T(8,128)(2,1)}, bf16[128,512]{1,0:T(8,128)(2,1)}, f32[128,16]{1,0:T(8,128)S(1)}) custom-call(bf16[8,1024,128]{2,1,0:T(8,128)(2,1)S(1)} %bitcast.74, f32[8,16]{1,0:T(8,128)S(1)} %fusion.13.weights_ref, bf16[4,256,128]{2,1,0:T(8,128)(2,1)S(1)} %get-tuple-element.49.state_ref, bf16[128,1024]{1,0:T(8,128)(2,1)S(1)} %copy-done.2, ...), custom_call_target="tpu_custom_call" | custom-call | flops 100663296 | bytes 3965504 | tf_op jit(solution)/shard_map/pallas_call | solution.py:51
  (111 shorter events, 6.8 us)
Async XLA Ops:
  7.2 88.8 %copy-start = (bf16[1,512,2048]{2,1,0:T(8,128)(2,1)S(1)}, bf16[1,512,2048]{2,1,0:T(8,128)(2,1)}, u32[]{:S(2)}) copy-start(bf16[1,512,2048]{2,1,0:T(8,128)(2,1)} %param.25) | copy-start | bytes 6291460
  7.2 62.8 %all-gather.11.cloned.1.call-start = ((), (), s32[]{:S(2)}) async-start(), calls=%async_computation.9 | async-start | bytes 2396160 | tf_op jit(solution)/shard_map/all_gather | solution.py:321
  15.3 106.9 %all-gather.7.cloned.1.call-start = ((), (), s32[]{:S(2)}) async-start(), calls=%async_computation.7 | async-start | bytes 4718592 | tf_op jit(solution)/shard_map/all_gather | solution.py:384
  17.6 1.0 copy-start.5
  18.6 1.0 copy-start.16
  20.7 43.7 %copy-start.22 = (bf16[128,384]{1,0:T(8,128)(2,1)}, bf16[128,384]{1,0:T(8,128)(2,1)S(1)}, u32[]{:S(2)}) copy-start(bf16[128,384]{1,0:T(8,128)(2,1)S(1)} %get-tuple-element.38.sel_ref) | copy-start | bytes 294916
  65.6 23.2 %all-to-all-start.1 = ((bf16[4,384,512]{2,1,0:T(8,128)(2,1)}), bf16[4,384,512]{2,1,0:T(8,128)(2,1)}, u32[]{:S(2)}, u32[]{:S(2)}) async-start(bf16[4,384,512]{2,1,0:T(8,128)(2,1)} %broadcast_in_dim.39), calls=%async_computation.1 | async-start | bytes 3145728 | tf_op jit(solution)/shard_map/all_to_all | solution.py:337
  90.1 23.2 %all-to-all-start.3 = ((bf16[4,384,512]{2,1,0:T(8,128)(2,1)}), bf16[4,384,512]{2,1,0:T(8,128)(2,1)}, u32[]{:S(2)}, u32[]{:S(2)}) async-start(bf16[4,384,512]{2,1,0:T(8,128)(2,1)} %broadcast_in_dim.40), calls=%async_computation.3 | async-start | bytes 3145728 | tf_op jit(solution)/shard_map/all_to_all | solution.py:337
  94.5 72.1 %all-gather.9.cloned.1.call-start = ((), (), s32[]{:S(2)}) async-start(), calls=%async_computation.8 | async-start | bytes 2359296 | tf_op jit(solution)/shard_map/all_gather | solution.py:386
  96.0 2.0 copy-start.28
  96.0 2.0 copy-start.30
  96.0 2.0 copy-start.32
  96.0 2.0 copy-start.34
  96.0 2.4 %copy-start.25 = (bf16[1,512,2048]{2,1,0:T(8,128)(2,1)S(1)}, bf16[1,512,2048]{2,1,0:T(8,128)(2,1)}, u32[]{:S(2)}) copy-start(bf16[1,512,2048]{2,1,0:T(8,128)(2,1)} %param.26) | copy-start | bytes 6291460
  98.4 1.9 copy-start.3
  98.4 2.1 copy-start.8
  98.4 2.1 copy-start.11
  98.4 2.1 copy-start.18
  102.2 15.9 %copy-start.12 = (f32[128,1024]{1,0:T(8,128)}, f32[128,1024]{1,0:T(8,128)S(1)}, u32[]{:S(2)}) copy-start(f32[128,1024]{1,0:T(8,128)S(1)} %get-tuple-element.47.out_ref) | copy-start | bytes 1572868
  113.3 2.1 copy-start.46
  113.3 2.2 copy-start.47
  114.9 3.2 %copy-start.36 = (bf16[384,512]{1,0:T(8,128)(2,1)}, bf16[384,512]{1,0:T(8,128)(2,1)S(1)}, u32[]{:S(2)}) copy-start(bf16[384,512]{1,0:T(8,128)(2,1)S(1)} %get-tuple-element.87) | copy-start | bytes 1179652
  114.9 3.2 %copy-start.38 = (bf16[384,512]{1,0:T(8,128)(2,1)}, bf16[384,512]{1,0:T(8,128)(2,1)S(1)}, u32[]{:S(2)}) copy-start(bf16[384,512]{1,0:T(8,128)(2,1)S(1)} %get-tuple-element.88) | copy-start | bytes 1179652
  114.9 3.2 %copy-start.40 = (bf16[384,512]{1,0:T(8,128)(2,1)}, bf16[384,512]{1,0:T(8,128)(2,1)S(1)}, u32[]{:S(2)}) copy-start(bf16[384,512]{1,0:T(8,128)(2,1)S(1)} %get-tuple-element.89) | copy-start | bytes 1179652
  114.9 3.2 %copy-start.42 = (bf16[384,512]{1,0:T(8,128)(2,1)}, bf16[384,512]{1,0:T(8,128)(2,1)S(1)}, u32[]{:S(2)}) copy-start(bf16[384,512]{1,0:T(8,128)(2,1)S(1)} %get-tuple-element.90) | copy-start | bytes 1179652
  118.2 1.0 copy-start.44
  118.2 1.9 copy-start.26
  122.2 99.2 %all-gather.13.cloned.1.call-start = ((), (), s32[]{:S(2)}) async-start(), calls=%async_computation.10 | async-start | bytes 2359296 | tf_op jit(solution)/shard_map/all_gather | solution.py:409
  145.2 20.2 %copy-start.6 = (bf16[128,2048]{1,0:T(8,128)(2,1)S(1)}, bf16[128,2048]{1,0:T(8,128)(2,1)}, u32[]{:S(2)}) copy-start(bf16[128,2048]{1,0:T(8,128)(2,1)} %g_ref.3) | copy-start | bytes 1572868
  174.0 3.0 %copy-start.13 = (f32[128,1024]{1,0:T(8,128)S(1)}, f32[128,1024]{1,0:T(8,128)}, u32[]{:S(2)}) copy-start(f32[128,1024]{1,0:T(8,128)} %copy-done.12) | copy-start | bytes 1572868
  180.9 35.2 %all-to-all-start.6 = ((bf16[128,8,256]{2,0,1:T(8,128)(2,1)}), bf16[128,8,256]{2,0,1:T(8,128)(2,1)}, u32[]{:S(2)}, u32[]{:S(2)}) async-start(bf16[128,8,256]{2,0,1:T(8,128)(2,1)} %bitcast.82), calls=%async_computation.6 | async-start | bytes 1048576 | tf_op jit(solution)/shard_map/all_to_all | solution.py:411
  188.0 4.4 %copy-start.29 = (bf16[384,512]{1,0:T(8,128)(2,1)S(1)}, bf16[384,512]{1,0:T(8,128)(2,1)}, u32[]{:S(2)}) copy-start(bf16[384,512]{1,0:T(8,128)(2,1)} %copy-done.28) | copy-start | bytes 1179652
  188.0 4.4 %copy-start.31 = (bf16[384,512]{1,0:T(8,128)(2,1)S(1)}, bf16[384,512]{1,0:T(8,128)(2,1)}, u32[]{:S(2)}) copy-start(bf16[384,512]{1,0:T(8,128)(2,1)} %copy-done.30) | copy-start | bytes 1179652
  188.0 4.4 %copy-start.33 = (bf16[384,512]{1,0:T(8,128)(2,1)S(1)}, bf16[384,512]{1,0:T(8,128)(2,1)}, u32[]{:S(2)}) copy-start(bf16[384,512]{1,0:T(8,128)(2,1)} %copy-done.32) | copy-start | bytes 1179652
  188.0 4.4 %copy-start.35 = (bf16[384,512]{1,0:T(8,128)(2,1)S(1)}, bf16[384,512]{1,0:T(8,128)(2,1)}, u32[]{:S(2)}) copy-start(bf16[384,512]{1,0:T(8,128)(2,1)} %copy-done.34) | copy-start | bytes 1179652
  188.0 4.4 %copy-start.45 = (bf16[384,512]{1,0:T(8,128)(2,1)S(1)}, bf16[384,512]{1,0:T(8,128)(2,1)}, u32[]{:S(2)}) copy-start(bf16[384,512]{1,0:T(8,128)(2,1)} %copy-done.44) | copy-start | bytes 1179652
  192.4 2.7 %copy-start.37 = (bf16[384,512]{1,0:T(8,128)(2,1)S(1)}, bf16[384,512]{1,0:T(8,128)(2,1)}, u32[]{:S(2)}) copy-start(bf16[384,512]{1,0:T(8,128)(2,1)} %copy-done.36) | copy-start | bytes 1179652
  192.4 2.7 %copy-start.39 = (bf16[384,512]{1,0:T(8,128)(2,1)S(1)}, bf16[384,512]{1,0:T(8,128)(2,1)}, u32[]{:S(2)}) copy-start(bf16[384,512]{1,0:T(8,128)(2,1)} %copy-done.38) | copy-start | bytes 1179652
  192.4 2.7 %copy-start.41 = (bf16[384,512]{1,0:T(8,128)(2,1)S(1)}, bf16[384,512]{1,0:T(8,128)(2,1)}, u32[]{:S(2)}) copy-start(bf16[384,512]{1,0:T(8,128)(2,1)} %copy-done.40) | copy-start | bytes 1179652
  192.4 2.7 %copy-start.43 = (bf16[384,512]{1,0:T(8,128)(2,1)S(1)}, bf16[384,512]{1,0:T(8,128)(2,1)}, u32[]{:S(2)}) copy-start(bf16[384,512]{1,0:T(8,128)(2,1)} %copy-done.42) | copy-start | bytes 1179652
  192.5 2.6 %copy-start.48 = (f32[384,512]{1,0:T(8,128)S(1)}, f32[384,512]{1,0:T(8,128)}, u32[]{:S(2)}) copy-start(f32[384,512]{1,0:T(8,128)} %fusion.10) | copy-start | bytes 2359300
  192.5 2.6 %copy-start.49 = (f32[384,512]{1,0:T(8,128)S(1)}, f32[384,512]{1,0:T(8,128)}, u32[]{:S(2)}) copy-start(f32[384,512]{1,0:T(8,128)} %fusion.4) | copy-start | bytes 2359300
  195.1 2.8 %copy-start.2 = (bf16[128,1024]{1,0:T(8,128)(2,1)S(1)}, bf16[128,1024]{1,0:T(8,128)(2,1)}, u32[]{:S(2)}) copy-start(bf16[128,1024]{1,0:T(8,128)(2,1)} %v_ref.5) | copy-start | bytes 786436
  195.1 2.8 %copy-start.10 = (bf16[128,512]{1,0:T(8,128)(2,1)S(1)}, bf16[128,512]{1,0:T(8,128)(2,1)}, u32[]{:S(2)}) copy-start(bf16[128,512]{1,0:T(8,128)(2,1)} %b_ref.5) | copy-start | bytes 393220
  195.1 2.8 %copy-start.20 = (f32[128,1024]{1,0:T(8,128)S(1)}, f32[128,1024]{1,0:T(8,128)}, u32[]{:S(2)}) copy-start(f32[128,1024]{1,0:T(8,128)} %copy-done.19) | copy-start | bytes 1572868
  203.0 18.4 %copy-start.24 = (f32[16]{0:T(128)S(1)}, f32[16]{0:T(128)}, u32[]{:S(2)}) copy-start(f32[16]{0:T(128)} %param.19) | copy-start | bytes 196
  221.4 1.6 copy-start.4
  223.0 1.0 copy-start.15
  (9 other events, 7.8 us)
Sparse Core Ops, SparseCore 0:
  15.4 40.7 all-gather.10
  57.8 45.4 all-gather.6
  122.3 28.7 all-gather.8
  180.0 41.3 all-gather.12
where the time goes:
time: 235 us; the launch traced here: 234 us
  blocking collectives  90 us (38%)
  waiting for transfers between devices  45.6 us (19%)
  matrix products  26.8 us (11%)
  local copies, waits for them, and re-layouts  24.9 us (11%)
  starting transfers between devices  16 us (7%)
  between operations  14.3 us (6%)
  Pallas kernels  13.6 us (6%)
  other arithmetic  2.78 us (1%)
    all_to_all x2, blocking collectives, over_sp(): lax.all_to_all(rows.reshape(experts, cap, width), 'sp', split_axis=0, con...  43.7 us
    all_to_all x2, waiting for transfers between devices, over_tp(): return lax.all_to_all(copies, 'tp', split_axis=0, concat_axis=0, tiled=True)  29.9 us
    dot_general x10, matrix products, mm(): return lax.dot_general(a, b, dims, preferred_element_type=F32)  25.7 us
    all_to_all x1, blocking collectives, body(): lax.all_to_all(shares, 'tp', split_axis=0, concat_axis=0, tiled=True)  21.3 us
    all_to_all x1, blocking collectives, body(): lax.all_to_all(reduced.reshape(experts, cap, width), 'sp', split_axis=0,...  17.7 us
    unnamed x104, local copies, waits for them, and re-layouts  16.8 us
    pallas_call x7, Pallas kernels, call(): pl.pallas_call(kernel, out_shape=outs, in_specs=[pl.BlockSpec(memory_spac...  13.6 us
    all_to_all x1, waiting for transfers between devices, body(): lax.all_to_all(stream_total, 'sp', split_axis=1, concat_axis=0, tiled=True)  13.1 us
  transfers between devices with their start and end apart: 7, of which 4 were waited for; matrix products, arithmetic and copies ran while one was open for 15% of the time, Pallas kernels for 3%

commit v1 on v0

v1 whole, which is shorter than its diff:
```python
import functools

import jax
import jax.numpy as jnp
from jax import lax
from jax.experimental import pallas as pl
from jax.experimental.pallas import tpu as pltpu
from jax.sharding import PartitionSpec as P

NSTATE = 128
CLAMP_LIMIT = 7.0
SIGMOID_SCALE = 1.702
HIGHEST = lax.Precision.HIGHEST
F32 = jnp.float32
BF16 = jnp.bfloat16
NN = (((1,), (0,)), ((), ()))
NT = (((1,), (1,)), ((), ()))
TN = (((0,), (0,)), ((), ()))
MESH = pl.DeviceIdType.MESH


def mm(a, b, dims=NN):
    return lax.dot_general(a, b, dims, preferred_element_type=F32)


def mm_exact(a, b, dims=NN):
    return lax.dot_general(a, b, dims, precision=HIGHEST, preferred_element_type=F32)


def grid_of(rows, cols):
    return (
        lax.broadcasted_iota(jnp.int32, (rows, cols), 0),
        lax.broadcasted_iota(jnp.int32, (rows, cols), 1),
    )


def spread(heads, size):
    at, col = grid_of(heads, heads * size)
    return ((col >= at * size) & (col < (at + 1) * size)).astype(F32)


def fold(heads, size):
    col, at = grid_of(heads * size, heads)
    return ((col >= at * size) & (col < (at + 1) * size)).astype(F32)


def out(shape, dtype):
    return jax.ShapeDtypeStruct(shape, dtype)


def mixing_of(log_ref, logt_ref, h):
    length = log_ref.shape[0]
    row, col = grid_of(length, length)
    gap = log_ref[:, h : h + 1] - logt_ref[h : h + 1, :]
    return jnp.where(row >= col, jnp.exp(jnp.minimum(gap, 0.0)), 0.0)


def local_part(groups, v_ref, b_ref, c_ref, steps_ref, log_ref, logt_ref, y_ref, state_ref):
    heads = steps_ref.shape[1]
    per, size = heads // groups, v_ref.shape[1] // heads
    wide = per * size
    length = v_ref.shape[0]
    expand = spread(heads, size)
    to_end = jnp.exp(log_ref[length - 1 :, :] - log_ref[...])
    x = v_ref[...].astype(F32) * mm_exact(steps_ref[...], expand)
    xe = (x * mm_exact(to_end, expand)).astype(BF16)
    x = x.astype(BF16)
    for g in range(groups):
        keys = b_ref[:, g * NSTATE : (g + 1) * NSTATE]
        scores = mm(c_ref[:, g * NSTATE : (g + 1) * NSTATE], keys, NT)
        parts = []
        for r in range(per):
            h = g * per + r
            att = (scores * mixing_of(log_ref, logt_ref, h)).astype(BF16)
            parts.append(mm(att, x[:, h * size : (h + 1) * size]))
        y_ref[:, g * wide : (g + 1) * wide] = jnp.concatenate(parts, axis=1)
        state_ref[g * wide : (g + 1) * wide, :] = mm(
            xe[:, g * wide : (g + 1) * wide], keys, TN
        ).astype(BF16)


def enter_part(groups, y_ref, gate_ref, c_ref, log_ref, state_ref, out_ref, gated_ref):
    heads = log_ref.shape[1]
    per, size = heads // groups, y_ref.shape[1] // heads
    wide = per * size
    decay = mm_exact(jnp.exp(log_ref[...]), spread(heads, size))
    for g in range(groups):
        at = slice(g * wide, (g + 1) * wide)
        entered = mm(c_ref[:, g * NSTATE : (g + 1) * NSTATE], state_ref[at, :], NT) * decay[:, at]
        mixed = y_ref[:, at] + entered
        out_ref[:, at] = mixed
        gate = gate_ref[:, at].astype(F32)
        gated_ref[:, at] = (mixed * gate * jax.nn.sigmoid(gate)).astype(BF16)


def gate_part(groups, grad_ref, out_ref, gate_ref, c_ref, log_ref, gate_grad_ref, mixer_ref, state_ref):
    heads = log_ref.shape[1]
    wide = grad_ref.shape[1] // groups
    decay = mm_exact(jnp.exp(log_ref[...]), spread(heads, grad_ref.shape[1] // heads))
    for g in range(groups):
        at = slice(g * wide, (g + 1) * wide)
        gate = gate_ref[:, at].astype(F32)
        sig = jax.nn.sigmoid(gate)
        grad = grad_ref[:, at]
        gate_grad_ref[:, at] = (grad * out_ref[:, at] * sig * (1.0 + gate * (1.0 - sig))).astype(BF16)
        mixer = grad * gate * sig
        mixer_ref[:, at] = mixer
        keys = c_ref[:, g * NSTATE : (g + 1) * NSTATE]
        state_ref[at, :] = mm((mixer * decay[:, at]).astype(BF16), keys, TN).astype(BF16)


def inner_part(
    groups, v_ref, b_ref, c_ref, steps_ref, log_ref, logt_ref, mixer_ref, state_ref,
    out_keys_ref, in_part_ref, x_part_ref, base_ref,
):
    heads = steps_ref.shape[1]
    per, size = heads // groups, v_ref.shape[1] // heads
    wide = per * size
    length = v_ref.shape[0]
    row, col = grid_of(length, length)
    later = (row <= col).astype(BF16)
    expand = spread(heads, size)
    mixer = mixer_ref[...]
    decayed = mixer * mm_exact(jnp.exp(log_ref[...]), expand)
    decayed_low = decayed.astype(BF16)
    mixer = mixer.astype(BF16)
    x = (v_ref[...].astype(F32) * mm_exact(steps_ref[...], expand)).astype(BF16)
    entering = []
    _, head_at = grid_of(length, heads)
    pairs = jnp.zeros((length, heads), F32)
    for g in range(groups):
        at = slice(g * wide, (g + 1) * wide)
        keys_in = b_ref[:, g * NSTATE : (g + 1) * NSTATE]
        keys_out = c_ref[:, g * NSTATE : (g + 1) * NSTATE]
        scores = mm(keys_out, keys_in, NT)
        score_grad = jnp.zeros((length, length), F32)
        parts = []
        for r in range(per):
            h = g * per + r
            here = slice(h * size, (h + 1) * size)
            mixing = mixing_of(log_ref, logt_ref, h)
            att = scores * mixing
            att_grad = mm(mixer[:, here], x[:, here], NT)
            parts.append(mm(att.astype(BF16), mixer[:, here], TN))
            score_grad = score_grad + att_grad * mixing
            after = mm(later, (att_grad * att).astype(BF16))
            crossing = jnp.sum(jnp.where(col < row, after, 0.0), axis=1, keepdims=True)
            pairs = pairs + jnp.where(head_at == h, crossing, 0.0)
        x_part_ref[:, at] = jnp.concatenate(parts, axis=1)
        score_grad = score_grad.astype(BF16)
        state = state_ref[at, :]
        out_keys_ref[:, g * NSTATE : (g + 1) * NSTATE] = (
            mm(score_grad, keys_in) + mm(decayed_low[:, at], state)
        ).astype(BF16)
        in_part_ref[:, g * NSTATE : (g + 1) * NSTATE] = mm(score_grad, keys_out, TN)
        entering.append(decayed[:, at] * mm(keys_out, state, NT))
    entering = jnp.concatenate(entering, axis=1)
    sums = mm_exact(entering, fold(heads, size))
    base_ref[...] = pairs + mm_exact((row <= col).astype(F32), sums)


def outer_part(
    groups, after_ref, state_ref, v_ref, b_ref, steps_ref, log_ref, rates_ref,
    in_part_ref, x_part_ref, base_ref, values_ref, in_keys_ref, steps_grad_ref,
):
    heads = steps_ref.shape[1]
    per, size = heads // groups, v_ref.shape[1] // heads
    wide = per * size
    length = v_ref.shape[0]
    row, col = grid_of(length, length)
    expand = spread(heads, size)
    last = log_ref[length - 1 :, :]
    steps = mm_exact(steps_ref[...], expand)
    to_end = mm_exact(jnp.exp(last - log_ref[...]), expand)
    values = v_ref[...].astype(F32)
    xe = values * steps * to_end
    xe_low = xe.astype(BF16)
    leaving, direct = [], []
    _, head_at = grid_of(1, heads)
    passing = jnp.zeros((1, heads), F32)
    for g in range(groups):
        at = slice(g * wide, (g + 1) * wide)
        keys_in = b_ref[:, g * NSTATE : (g + 1) * NSTATE]
        for r in range(per):
            h = g * per + r
            here = slice(h * size, (h + 1) * size)
            both = after_ref[here, :] * state_ref[here, :].astype(F32)
            both = jnp.sum(jnp.sum(both, axis=0, keepdims=True), axis=1, keepdims=True)
            passing = passing + jnp.where(head_at == h, both, 0.0)
        after = after_ref[at, :].astype(BF16)
        reached = mm(keys_in, after, NT)
        x_grad = x_part_ref[:, at] + reached * to_end[:, at]
        values_ref[:, at] = (x_grad * steps[:, at]).astype(BF16)
        in_keys_ref[:, g * NSTATE : (g + 1) * NSTATE] = (
            in_part_ref[:, g * NSTATE : (g + 1) * NSTATE] + mm(xe_low[:, at], after)
        ).astype(BF16)
        leaving.append(reached * xe[:, at])
        direct.append(x_grad * values[:, at])
    gather = fold(heads, size)
    leaving = mm_exact(jnp.concatenate(leaving, axis=1), gather)
    direct = mm_exact(jnp.concatenate(direct, axis=1), gather)
    crossing = base_ref[...] + mm_exact((col < row).astype(F32), leaving) + jnp.exp(last) * passing
    steps_grad_ref[...] = direct - rates_ref[...] * crossing


class Sends:
    def __init__(self, sems):
        self.sems, self.used, self.open = sems, 0, []

    def copy(self, src, dst, landed, to):
        sem = self.sems.at[self.used]
        self.used += 1
        return pltpu.make_async_remote_copy(
            src_ref=src, dst_ref=dst, send_sem=sem, recv_sem=landed,
            device_id=to, device_id_type=MESH,
        )

    def send(self, cond, src, dst, landed, to):
        copy = self.copy(src, dst, landed, to)
        when(cond, copy.start)
        self.open.append((cond, copy))

    def finish(self):
        assert self.used <= self.sems.shape[0]
        for cond, copy in self.open:
            when(cond, copy.wait_send)


def when(cond, action):
    if cond is None:
        action()
    else:
        pl.when(cond)(action)


def both(a, b):
    return a if b is None else b if a is None else a & b


class Place:
    def __init__(self, n, m):
        self.n, self.m, self.chips = n, m, n // 2
        self.s, self.t = lax.axis_index("sp"), lax.axis_index("tp")
        self.z, self.c = self.s // 2, lax.rem(self.s, 2)
        self.mate = self.z * 2 + 1 - self.c

    def around(self):
        for d in range(1, self.chips):
            for sign in (1, -1):
                at = self.z + sign * d
                yield d, at, (at >= 0) & (at < self.chips)

    def planes(self):
        for d in range(1, self.m):
            yield lax.rem(self.t + d, self.m)


class Line:
    def __init__(self, place, sends, own, full, landed):
        self.p, self.sends, self.own, self.full, self.landed = place, sends, own, full, landed

    def put(self, cond, src, owner, to):
        self.sends.send(cond, src, self.full.at[owner], self.landed.at[owner], (to, self.p.t))

    def arrived(self, cond, owner):
        block = self.full.at[owner]
        copy = pltpu.make_async_remote_copy(
            src_ref=block, dst_ref=block, send_sem=self.landed.at[owner], recv_sem=self.landed.at[owner],
            device_id=(self.p.mate, self.p.t), device_id_type=MESH,
        )
        when(cond, copy.wait_recv)

    def begin(self, up=True, down=True):
        p = self.p
        if down:
            self.put(p.z > 0, self.own, p.s, p.s - 2)
            self.put(None, self.own, p.s, p.mate)
        if up:
            self.put(p.z < p.chips - 1, self.own, p.s, p.s + 2)

    def step(self, d):
        p = self.p
        below, above = p.s - 2 * d, p.s + 2 * d
        from_below, from_above = p.z >= d, p.z + d < p.chips
        self.arrived(from_below, below)
        if d < p.chips - 1:
            self.put(from_below & (p.z < p.chips - 1), self.full.at[below], below, p.s + 2)
        self.put(from_below, self.full.at[below], below, p.mate)
        self.arrived(from_above, above)
        if d < p.chips - 1:
            self.put(from_above & (p.z > 0), self.full.at[above], above, p.s - 2)
        self.put(from_above, self.full.at[above], above, p.mate)

    def end(self):
        for k in range(self.p.chips):
            self.arrived(None, 2 * k + 1 - self.p.c)


class Chain:
    def __init__(self, place, sends, first, own, mates, span, mate_span, carry, onward, landed, swapped):
        self.p, self.sends, self.first = place, sends, first
        self.own, self.mates, self.span, self.mate_span = own, mates, span, mate_span
        self.carry, self.onward, self.landed, self.swapped = carry, onward, landed, swapped
        self.starts = place.z == (0 if first == 0 else place.chips - 1)
        self.stops = place.z == (place.chips - 1 if first == 0 else 0)
        self.next = place.s + (2 if first == 0 else -2)

    def wait(self, cond, ref, sem):
        copy = pltpu.make_async_remote_copy(
            src_ref=ref, dst_ref=ref, send_sem=sem, recv_sem=sem,
            device_id=(self.p.mate, self.p.t), device_id_type=MESH,
        )
        when(cond, copy.wait_recv)

    def exchange(self):
        p = self.p
        self.sends.send(None, self.own, self.mates, self.swapped, (p.mate, p.t))

    def step(self, heads, size, only=None):
        p, c = self.p, self.p.c
        half = heads // 2
        rows = half * size

        def zero():
            self.carry[...] = jnp.zeros(self.carry.shape, self.carry.dtype)

        when(both(self.starts, only), zero)
        self.wait(both(~self.starts, only), self.carry.at[c], self.landed.at[0])
        self.sends.send(
            both(~self.starts, only), self.carry.at[c], self.carry.at[c], self.landed.at[1], (p.mate, p.t)
        )

        def advance():
            mine, other = jnp.exp(self.span[0:1, :]), jnp.exp(self.mate_span[0:1, :])
            near = c == self.first
            for r in range(half):
                at = pl.ds(pl.multiple_of(c * rows + r * size, size), size)
                low, high = slice(r, r + 1), slice(half + r, half + r + 1)
                w_mine = jnp.where(c == 0, mine[:, low], mine[:, high])
                w_other = jnp.where(c == 0, other[:, low], other[:, high])
                own, mate = self.own[at, :].astype(F32), self.mates[at, :].astype(F32)
                carried = self.carry[c, r * size : (r + 1) * size, :].astype(F32)
                a = jnp.where(near, w_mine, w_other) * carried + jnp.where(near, own, mate)
                b = jnp.where(near, w_other, w_mine) * a + jnp.where(near, mate, own)
                self.onward[r * size : (r + 1) * size, :] = b.astype(BF16)

        go = both(~self.stops, only)
        when(go, advance)
        self.sends.send(go, self.onward, self.carry.at[c], self.landed.at[0], (self.next, p.t))

    def finish(self, heads, size, target):
        p = self.p
        half = heads // 2
        rows = half * size
        self.wait(~self.starts, self.carry.at[1 - p.c], self.landed.at[1])
        other = jnp.exp(self.mate_span[0:1, :])
        near = p.c == self.first
        for h in range(heads):
            at = slice(h * size, (h + 1) * size)
            inside = slice((h % half) * size, (h % half + 1) * size)
            carried = self.carry[h // half, inside, :].astype(F32)
            through = other[:, h : h + 1] * carried + self.mates[at, :].astype(F32)
            target[at, :] = jnp.where(near, carried, through).astype(target.dtype)


def comm_kernel(
    cfg,
    v_ref, gate_ref, b_ref, c_ref, steps_ref, rates_ref, proj_ref, x_ref, g_ref, routes_ref, weights_ref,
    wg_hbm, wu_hbm, wd_hbm,
    dg_hbm, du_hbm, dd_hbm, grad_gate_ref, out_keys_ref, in_part_ref, x_part_ref, base_ref, log_ref,
    state_in, after_ref, all_stream, all_gated,
    wg, wu, wd, dw, logt_ref, y_ref, mixer_out, gated, own_state, mate_state, own_grad, mate_grad,
    span, mate_span, carry_f, onward_f, carry_b, onward_b, gated_grad, mixer_grad,
    picked_ref, parts, local, rows, act, gate_g, up_g, back, shares, reduced, returned, stream, full_proj,
    send_sems, load_sems, store_sems, dz_in, dp_in, rs_in, rt_in, st_in, as_in, proj_in, gated_in,
    fwd_in, bwd_in, swap_in,
):
    n, m, groups, capp, width, share = cfg
    p = Place(n, m)
    sends = Sends(send_sems)
    tokens, top = routes_ref.shape
    heads = steps_ref.shape[1]
    size = v_ref.shape[1] // heads
    slots = n * capp
    model = x_ref.shape[1]
    hidden = wg.shape[0]

    def wait(cond, ref, sem):
        copy = pltpu.make_async_remote_copy(
            src_ref=ref, dst_ref=ref, send_sem=sem, recv_sem=sem,
            device_id=(p.mate, p.t), device_id_type=MESH,
        )
        when(cond, copy.wait_recv)

    loads = [
        pltpu.make_async_copy(src, dst, load_sems.at[k])
        for k, (src, dst) in enumerate(((wg_hbm, wg), (wu_hbm, wu), (wd_hbm, wd)))
    ]
    for load in loads:
        load.start()
    barrier = pltpu.get_barrier_semaphore()
    for d in range(1, n):
        pl.semaphore_signal(barrier, inc=1, device_id=(lax.rem(p.s + d, n), p.t), device_id_type=MESH)
    for other in p.planes():
        pl.semaphore_signal(barrier, inc=1, device_id=(p.s, other), device_id_type=MESH)

    row, col = grid_of(tokens, tokens)
    drop = -steps_ref[...] * rates_ref[...]
    log = mm_exact((row >= col).astype(F32), drop)
    log_ref[...] = log
    logt_ref[...] = log.T
    span[...] = jnp.zeros(span.shape, F32)
    span[0:1, 0:heads] = log[tokens - 1 :, :]
    local_part(groups, v_ref, b_ref, c_ref, steps_ref, log_ref, logt_ref, y_ref, own_state)

    start = pl.multiple_of(p.t * width, 128)
    mine = pl.ds(start, width)
    _, expert = grid_of(tokens, n)
    _, slot = grid_of(tokens, slots)
    _, near = grid_of(tokens, 2 * capp)
    near = jnp.where(near < capp, p.s * capp + near, p.mate * capp + near - capp)
    hits = [expert == routes_ref[:, k : k + 1] for k in range(top)]
    named = sum(hit.astype(F32) for hit in hits)
    before = mm((row > col).astype(BF16), named.astype(BF16))
    every = jnp.zeros((tokens, slots), F32)
    every_near = jnp.zeros((tokens, 2 * capp), F32)
    grads = jnp.zeros((slots, width), F32)
    grads_near = jnp.zeros((2 * capp, model), F32)
    g_part = g_ref[:, mine].astype(F32)
    for k in range(top):
        rank = jnp.sum(jnp.where(hits[k], before, 0.0), axis=1, keepdims=True).astype(jnp.int32)
        at = routes_ref[:, k : k + 1] * capp + rank
        chosen = (slot == at).astype(F32)
        chosen_near = (near == at).astype(F32)
        every, every_near = every + chosen, every_near + chosen_near
        weight = weights_ref[:, k : k + 1]
        grads = grads + mm(chosen.astype(BF16), (g_part * weight).astype(BF16), TN)
        grads_near = grads_near + mm(
            chosen_near.astype(BF16), (g_ref[...].astype(F32) * weight).astype(BF16), TN
        )
    picked = every.astype(BF16)
    picked_ref[...] = picked
    parts[0] = mm(picked, x_ref[:, mine], TN).astype(BF16).reshape(n, capp, width)
    parts[1] = grads.astype(BF16).reshape(n, capp, width)
    x_near = mm(every_near.astype(BF16), x_ref[...], TN).astype(BF16)
    grads_near = grads_near.astype(BF16)
    local[0] = x_near[capp:]
    local[1] = grads_near[capp:]

    pl.semaphore_wait(barrier, n + m - 2)
    sends.send(None, local, rows.at[:, p.s], dz_in.at[p.s], (p.mate, p.t))
    forward = Chain(
        p, sends, 0, own_state, mate_state, span, mate_span, carry_f, onward_f, fwd_in, swap_in.at[0]
    )
    forward.exchange()
    sends.send(None, span, mate_span, swap_in.at[2], (p.mate, p.t))
    wait(None, mate_state, swap_in.at[0])
    wait(None, mate_span, swap_in.at[2])
    forward.step(heads, size, only=p.z == 0)
    for _, at, ok in p.around():
        for core in range(2):
            to = at * 2 + core
            sends.send(ok, parts.at[:, to], rows.at[:, p.s, :, mine], dz_in.at[p.s], (to, p.t))
    rows[0, p.s] = x_near[:capp]
    rows[1, p.s] = grads_near[:capp]
    line = Line(p, sends, proj_ref, full_proj, proj_in)
    line.begin(up=False)
    full_proj[p.s] = proj_ref[...]

    for d in range(1, p.chips):
        for sign in (1, -1):
            at = p.z + sign * d
            ok = (at >= 0) & (at < p.chips)
            for core in range(2):
                source = at * 2 + core
                wait(ok, rows.at[:, source, :, mine], dz_in.at[source])
            block = rows.at[:, pl.ds(2 * at, 2), :, mine]
            for other in p.planes():
                sends.send(ok, block, block, dp_in.at[at, p.t], (p.s, other))
        forward.step(heads, size, only=p.z == d)
    line.begin(down=False)
    forward.finish(heads, size, state_in)
    enter_part(groups, y_ref, gate_ref, c_ref, log_ref, state_in, mixer_out, gated)
    all_gated[p.s] = gated[...]
    line.step(1)
    wait(None, rows.at[:, p.mate], dz_in.at[p.mate])
    for _, at, ok in p.around():
        for other in p.planes():
            wait(ok, rows.at[:, pl.ds(2 * at, 2), :, pl.ds(pl.multiple_of(other * width, 128), width)], dp_in.at[at, other])

    for load in loads:
        load.wait()
    chunk = min(256, hidden)

    def experts(k, _):
        at = pl.ds(pl.multiple_of(k * chunk, chunk), chunk)
        in_rows = rows[0].reshape(slots, model)
        gate_pre = mm(in_rows, wg[at, :], NT)
        up_pre = mm(in_rows, wu[at, :], NT)
        act_grad = mm(rows[1].reshape(slots, model), wd[at, :], NT)
        gate_clamped = jnp.minimum(gate_pre, CLAMP_LIMIT)
        up_clamped = jnp.clip(up_pre, -CLAMP_LIMIT, CLAMP_LIMIT) + 1.0
        sig = jax.nn.sigmoid(SIGMOID_SCALE * gate_clamped)
        swish = gate_clamped * sig
        act[:, at] = (up_clamped * swish).astype(BF16)
        gate_g[:, at] = jnp.where(
            gate_pre < CLAMP_LIMIT,
            act_grad * up_clamped * sig * (1.0 + SIGMOID_SCALE * gate_clamped * (1.0 - sig)),
            0.0,
        ).astype(BF16)
        up_g[:, at] = jnp.where(jnp.abs(up_pre) < CLAMP_LIMIT, act_grad * swish, 0.0).astype(BF16)
        return 0

    lax.fori_loop(0, hidden // chunk, experts, 0)

    def backs(q, _):
        at = pl.ds(pl.multiple_of(q * width, 128), width)
        back[q] = (mm(gate_g[...], wg[:, at]) + mm(up_g[...], wu[:, at])).astype(BF16)
        return 0

    lax.fori_loop(0, m, backs, 0)
    pair = 2 * capp
    chunks = [lax.rem(p.z + d, p.chips) for d in range(1, p.chips + 1)]
    spans = [pl.ds(pl.multiple_of(at * pair, pair), pair) for at in chunks]
    for at, here in zip(chunks, spans):
        for other in p.planes():
            sends.send(None, back.at[other, here], shares.at[p.t, here], rs_in.at[at, p.t], (p.s, other))

    def weight_grads(k, _):
        at = pl.ds(pl.multiple_of(k * chunk, chunk), chunk)
        in_rows = rows[0].reshape(slots, model)
        dw[0, at, :] = mm(gate_g[:, at], in_rows, TN).astype(BF16)
        dw[1, at, :] = mm(up_g[:, at], in_rows, TN).astype(BF16)
        dw[2, at, :] = mm(act[:, at], rows[1].reshape(slots, model), TN).astype(BF16)
        return 0

    lax.fori_loop(0, hidden // chunk, weight_grads, 0)
    stores = [
        pltpu.make_async_copy(dw.at[k], dst, store_sems.at[k]) for k, dst in enumerate((dg_hbm, du_hbm, dd_hbm))
    ]
    for store in stores:
        store.start()
    if p.chips > 2:
        line.step(2)
    for k, (at, here) in enumerate(zip(chunks, spans)):
        total = back[p.t, here].astype(F32)
        for other in p.planes():
            wait(None, shares.at[other, here], rs_in.at[at, other])
            total = total + shares[other, here].astype(F32)
        reduced[pl.ds(2 * at, 2)] = total.astype(BF16).reshape(2, capp, width)
        if k < p.chips - 1:
            for core in range(2):
                to = 2 * at + core
                sends.send(None, reduced.at[to], returned.at[p.s], rt_in.at[p.s], (to, p.t))
        else:
            sends.send(None, reduced.at[p.mate], returned.at[p.s], rt_in.at[p.s], (p.mate, p.t))
            returned[p.s] = reduced[p.s]
    gather = Line(p, sends, gated, all_gated, gated_in)
    gather.begin()
    for d in range(3, p.chips):
        line.step(d)
    for d in range(1, n):
        source = lax.rem(p.s + d, n)
        wait(None, returned.at[source], rt_in.at[source])
    stream[:, mine] = (g_ref[:, mine].astype(F32) + mm(picked_ref[...], returned[...].reshape(slots, width))).astype(BF16)
    for other in p.planes():
        sends.send(None, stream.at[:, mine], stream.at[:, mine], st_in.at[p.t], (p.s, other))
    line.end()
    gather.step(1)
    for other in p.planes():
        wait(None, stream.at[:, pl.ds(pl.multiple_of(other * width, 128), width)], st_in.at[other])
    step = max(share, 128)

    def columns(j):
        return pl.ds(pl.multiple_of(j * share // step * step, 128), step)

    def to_all():
        for _, at, ok in p.around():
            for core in range(2):
                to = at * 2 + core
                sends.send(ok, stream.at[:, columns(to)], all_stream.at[p.s], as_in.at[p.s], (to, p.t))
        sends.send(None, stream.at[:, columns(p.mate)], all_stream.at[p.s], as_in.at[p.s], (p.mate, p.t))
        all_stream[p.s] = stream[:, columns(p.s)]

    to_all()
    gated_grad[...] = mm(stream[...], full_proj[...].reshape(model, v_ref.shape[1]))
    gate_part(groups, gated_grad, mixer_out, gate_ref, c_ref, log_ref, grad_gate_ref, mixer_grad, own_grad)
    backward = Chain(
        p, sends, 1, own_grad, mate_grad, span, mate_span, carry_b, onward_b, bwd_in, swap_in.at[1]
    )
    backward.exchange()
    wait(None, mate_grad, swap_in.at[1])
    backward.step(heads, size, only=p.z == p.chips - 1)
    inner_part(
        groups, v_ref, b_ref, c_ref, steps_ref, log_ref, logt_ref, mixer_grad, state_in,
        out_keys_ref, in_part_ref, x_part_ref, base_ref,
    )
    for d in range(1, p.chips):
        if d > 1:
            gather.step(d)
        backward.step(heads, size, only=p.z == p.chips - 1 - d)
    backward.finish(heads, size, after_ref)
    gather.end()
    for d in range(1, n):
        source = lax.rem(p.s + d, n)
        wait(None, all_stream.at[source], as_in.at[source])
    for store in stores:
        store.wait()
    sends.finish()


def last_kernel(
    cfg,
    dg_in, du_in, dd_in, grad_gate_in, out_keys_in, in_part_ref, x_part_ref, base_ref, log_ref,
    state_in, after_ref, all_stream, all_gated, v_ref, b_ref, steps_ref, rates_ref,
    dg_out, du_out, dd_out, proj_grad_ref, values_ref, grad_gate_ref, in_keys_ref, out_keys_ref, steps_grad_ref,
    passing, sums, sems,
):
    n, m, groups, capp, width, share = cfg
    ins = [pltpu.make_async_copy(src, passing.at[k], sems.at[k]) for k, src in enumerate((dg_in, du_in, dd_in))]
    outs = [pltpu.make_async_copy(passing.at[k], dst, sems.at[3 + k]) for k, dst in enumerate((dg_out, du_out, dd_out))]
    for copy in ins:
        copy.start()
    tokens = all_stream.shape[0] * all_stream.shape[1]
    step = all_stream.shape[2]
    grad = mm(all_stream[...].reshape(tokens, step), all_gated[...].reshape(tokens, all_gated.shape[2]), TN)
    if step == share:
        proj_grad_ref[...] = grad
    else:
        sums[...] = grad
        off = pl.multiple_of(lax.rem(lax.axis_index("sp"), step // share) * share, share)
        proj_grad_ref[...] = sums[pl.ds(off, share), :]
    for a, b in zip(ins, outs):
        a.wait()
        b.start()
    grad_gate_ref[...] = grad_gate_in[...]
    out_keys_ref[...] = out_keys_in[...]
    outer_part(
        groups, after_ref, state_in, v_ref, b_ref, steps_ref, log_ref, rates_ref,
        in_part_ref, x_part_ref, base_ref, values_ref, in_keys_ref, steps_grad_ref,
    )
    for copy in outs:
        copy.wait()


def body(
    mix_values, mix_gate, input_keys, output_keys, step_sizes, decay_rates, out_proj, expert_inputs,
    stream_grad, routes, route_weights, gate_proj, up_proj, down_proj,
):
    tokens, inner = mix_values.shape
    model = stream_grad.shape[1]
    top = routes.shape[1]
    n, m = lax.axis_size("sp"), lax.axis_size("tp")
    experts = gate_proj.shape[0] * n
    cap = 3 * tokens * top // (2 * experts)
    capp = -(-cap // 16) * 16
    slots = n * capp
    heads = step_sizes.shape[1]
    groups = input_keys.shape[1] // NSTATE
    width = model // m
    hidden = gate_proj.shape[1]
    share = model // n
    chips = n // 2
    step = max(share, 128)
    rates = decay_rates.reshape(1, heads)
    cfg = (n, m, groups, capp, width, share)
    vm, anyw = pl.BlockSpec(memory_space=pltpu.VMEM), pl.BlockSpec(memory_space=pl.ANY)
    keys_shape = input_keys.shape
    weight = (hidden, model)
    dma = pltpu.SemaphoreType.DMA
    sent = (
        3 + 1 + 4 * (chips - 1) + 2 * (chips - 1) * (m - 1) + 2 * (3 + 4 * (chips - 1))
        + chips * (m - 1) + 2 * chips + (m - 1) + 4 * chips + 2 * 2 * (chips + 1) + 8
    )
    mids = pl.pallas_call(
        functools.partial(comm_kernel, cfg),
        out_shape=[
            out(weight, BF16), out(weight, BF16), out(weight, BF16),
            out((tokens, inner), BF16), out(keys_shape, BF16), out(keys_shape, F32),
            out((tokens, inner), F32), out((tokens, heads), F32), out((tokens, heads), F32),
            out((inner, NSTATE), BF16), out((inner, NSTATE), F32),
            out((n, tokens, step), BF16), out((n, tokens, inner), BF16),
        ],
        in_specs=[vm] * 11 + [anyw] * 3,
        out_specs=[anyw] * 3 + [vm] * 10,
        scratch_shapes=[
            pltpu.VMEM(weight, BF16), pltpu.VMEM(weight, BF16), pltpu.VMEM(weight, BF16),
            pltpu.VMEM((3,) + weight, BF16),
            pltpu.VMEM((heads, tokens), F32),
            pltpu.VMEM((tokens, inner), F32), pltpu.VMEM((tokens, inner), F32), pltpu.VMEM((tokens, inner), BF16),
            pltpu.VMEM((inner, NSTATE), BF16), pltpu.VMEM((inner, NSTATE), BF16),
            pltpu.VMEM((inner, NSTATE), BF16), pltpu.VMEM((inner, NSTATE), BF16),
            pltpu.VMEM((8, 128), F32), pltpu.VMEM((8, 128), F32),
            pltpu.VMEM((2, inner // 2, NSTATE), BF16), pltpu.VMEM((inner // 2, NSTATE), BF16),
            pltpu.VMEM((2, inner // 2, NSTATE), BF16), pltpu.VMEM((inner // 2, NSTATE), BF16),
            pltpu.VMEM((tokens, inner), F32), pltpu.VMEM((tokens, inner), F32),
            pltpu.VMEM((tokens, slots), BF16),
            pltpu.VMEM((2, n, capp, width), BF16),
            pltpu.VMEM((2, capp, model), BF16),
            pltpu.VMEM((2, n, capp, model), BF16),
            pltpu.VMEM((slots, hidden), BF16), pltpu.VMEM((slots, hidden), BF16), pltpu.VMEM((slots, hidden), BF16),
            pltpu.VMEM((m, slots, width), BF16), pltpu.VMEM((m, slots, width), BF16),
            pltpu.VMEM((n, capp, width), BF16), pltpu.VMEM((n, capp, width), BF16),
            pltpu.VMEM((tokens, model), BF16),
            pltpu.VMEM((n,) + out_proj.shape, BF16),
            dma((sent,)), dma((3,)), dma((3,)),
            dma((n,)), dma((chips, m)), dma((chips, m)), dma((n,)), dma((m,)), dma((n,)), dma((n,)), dma((n,)),
            dma((2,)), dma((2,)), dma((3,)),
        ],
        cost_estimate=pl.CostEstimate(flops=10**10, bytes_accessed=3 * 10**7, transcendentals=0),
        compiler_params=pltpu.CompilerParams(
            collective_id=0, has_side_effects=True, vmem_limit_bytes=60 * 2**20
        ),
    )(
        mix_values, mix_gate, input_keys, output_keys, step_sizes, rates, out_proj, expert_inputs,
        stream_grad, routes, route_weights,
        gate_proj.reshape(weight), up_proj.reshape(weight), down_proj.reshape(weight),
    )
    log = mids[8]
    outs = pl.pallas_call(
        functools.partial(last_kernel, cfg),
        out_shape=[
            out(weight, BF16), out(weight, BF16), out(weight, BF16),
            out((share, inner), F32), out((tokens, inner), BF16), out((tokens, inner), BF16),
            out(keys_shape, BF16), out(keys_shape, BF16), out((tokens, heads), F32),
        ],
        in_specs=[anyw] * 3 + [vm] * 14,
        out_specs=[anyw] * 3 + [vm] * 6,
        scratch_shapes=[pltpu.VMEM((3,) + weight, BF16), pltpu.VMEM((step, inner), F32), dma((6,))],
        cost_estimate=pl.CostEstimate(flops=10**9, bytes_accessed=2 * 10**7, transcendentals=0),
        compiler_params=pltpu.CompilerParams(vmem_limit_bytes=40 * 2**20),
    )(*mids, mix_values, input_keys, step_sizes, rates)
    shape = gate_proj.shape
    return tuple(o.reshape(shape) for o in outs[:3]) + tuple(outs[3:])


def solution(mesh):
    return jax.shard_map(
        body,
        mesh=mesh,
        in_specs=(
            P("sp", "tp"), P("sp", "tp"), P("sp", "tp"), P("sp", "tp"), P("sp", "tp"), P("tp"),
            P("sp", "tp"), P("sp", None), P("sp", None), P("sp", None), P("sp", None),
            P("sp", "tp", None), P("sp", "tp", None), P("sp", "tp", None),
        ),
        out_specs=(
            P("sp", "tp", None), P("sp", "tp", None), P("sp", "tp", None),
            P("sp", "tp"), P("sp", "tp"), P("sp", "tp"), P("sp", "tp"), P("sp", "tp"), P("sp", "tp"),
        ),
        check_vma=False,
    )
```

time: 235 us -> 139 us (0.59)
  Pallas kernels: 13.6 us -> 117 us
  blocking collectives: 90 us -> 0 us
  waiting for transfers between devices: 45.6 us -> 0 us
  matrix products: 26.8 us -> 0 us
  starting transfers between devices: 16 us -> 0 us
  between operations: 14.3 us -> 0.72 us
  local copies, waits for them, and re-layouts: 24.9 us -> 19.8 us
  other arithmetic: 2.78 us -> 0 us
    pallas_call x7 -> x2, Pallas kernels: 13.6 us -> 117 us  [the longest x1 111 us: body(): pl.pallas_call(functools.partial(comm_kernel, cfg), out_shape=[out(weight...]
    all_to_all x4 -> x0, blocking collectives: 82.6 us -> none  [the longest x2 43.7 us: over_sp(): lax.all_to_all(rows.reshape(experts, cap, width), 'sp', split_axis=0, con...]
    all_to_all x3 -> x0, waiting for transfers between devices: 43 us -> none  [the longest x2 29.9 us: over_tp(): return lax.all_to_all(copies, 'tp', split_axis=0, concat_axis=0, tiled=True)]
    dot_general x13 -> x0, matrix products: 26.8 us -> none  [the longest x10 25.7 us: mm(): return lax.dot_general(a, b, dims, preferred_element_type=F32)]
    all_to_all x3 -> x0, starting transfers between devices: 15.8 us -> none  [the longest x2 8.73 us: over_tp(): return lax.all_to_all(copies, 'tp', split_axis=0, concat_axis=0, tiled=True)]
    all_gather x1 -> x0, blocking collectives: 7.4 us -> none  [body(): stream_total = lax.all_gather(stream_part, 'tp', axis=1, tiled=True)]
    unnamed x104 -> x38, local copies, waits for them, and re-layouts: 16.8 us -> 19.8 us
    squeeze x2 -> x0, local copies, waits for them, and re-layouts: 3.06 us -> none  [side_by_side(): stacked[c]]
  transfers between devices with their start and end apart: 7 -> 0, of which waited for: 4 -> 0; matrix products, arithmetic and copies ran while one was open for 15% -> 0% of each run, Pallas kernels for 3% -> 0%
where the time goes in v1:
time: 139 us; the launch traced here: 138 us
  Pallas kernels  117 us (84%)
  local copies, waits for them, and re-layouts  19.8 us (14%)
    pallas_call x1, Pallas kernels, body(): pl.pallas_call(functools.partial(comm_kernel, cfg), out_shape=[out(weight...  111 us
    unnamed x38, local copies, waits for them, and re-layouts  19.8 us
    pallas_call x1, Pallas kernels, body(): pl.pallas_call(functools.partial(last_kernel, cfg), out_shape=[out(weight...  5.98 us

profile of v1, /device:TPU:1, one launch (start us, length us, event | category | flops | bytes accessed | tf_op | source)
XLA Modules:
  0.0 137.8 jit_solution(5851342829571221341)
XLA Ops:
  0.6 1.4 %copy.23.steps_ref = f32[128,16]{1,0:T(8,128)} copy(f32[128,16]{0,1:T(8,128)} %param.18) | data formatting | bytes 16384 | tf_op args[4]
  2.1 1.4 %copy.24.routes_ref = s32[128,2]{1,0:T(8,128)} copy(s32[128,2]{0,1:T(2,128)} %param.23) | data formatting | bytes 2048 | tf_op args[9]
  3.5 1.4 %copy.25.weights_ref = f32[128,2]{1,0:T(8,128)} copy(f32[128,2]{0,1:T(2,128)} %param.24) | data formatting | bytes 2048 | tf_op args[10]
  4.9 0.0 copy-start.7
  4.9 0.0 copy-start.8
  4.9 0.0 copy-start.12
  4.9 0.0 copy-start.16
  4.9 111.3 %shard_map.205 = (bf16[512,2048]{1,0:T(8,128)(2,1)}, bf16[512,2048]{1,0:T(8,128)(2,1)}, bf16[512,2048]{1,0:T(8,128)(2,1)}, bf16[128,1024]{1,0:T(8,128)(2,1)}, bf...) custom-call(bf16[128,1024]{1,0:T(8,128)(2,1)} %v_ref.3, ...), custom_call_target="tpu_custom_call" | custom-call | flops 10000000000 | bytes 30000000 | tf_op jit(solution)/shard_map/pallas_call | solution.py:675
  116.2 0.0 copy-done.7
  116.2 0.0 copy-done.8
  116.2 0.0 copy-done.12
  116.2 0.0 copy-done.16
  116.2 0.0 copy-start
  116.2 1.6 %copy-done = bf16[512,2048]{1,0:T(8,128)(2,1)S(1)} copy-done((bf16[512,2048]{1,0:T(8,128)(2,1)S(1)}, bf16[512,2048]{1,0:T(8,128)(2,1)}, u32[]{:S(2)}) %copy-start) | copy-done | bytes 2097176
  117.8 0.0 copy-start.1
  117.8 1.6 %copy-done.1 = bf16[512,2048]{1,0:T(8,128)(2,1)S(1)} copy-done((bf16[512,2048]{1,0:T(8,128)(2,1)S(1)}, bf16[512,2048]{1,0:T(8,128)(2,1)}, u32[]{:S(2)}) %copy-start.1) | copy-done | bytes 2097176
  119.4 0.0 copy-start.2
  119.4 1.6 %copy-done.2 = bf16[512,2048]{1,0:T(8,128)(2,1)S(1)} copy-done((bf16[512,2048]{1,0:T(8,128)(2,1)S(1)}, bf16[512,2048]{1,0:T(8,128)(2,1)}, u32[]{:S(2)}) %copy-start.2) | copy-done | bytes 2097176
  121.0 0.0 copy-start.3
  121.0 1.6 %copy-done.3 = bf16[8,128,1024]{2,1,0:T(8,128)(2,1)S(1)} copy-done((bf16[8,128,1024]{2,1,0:T(8,128)(2,1)S(1)}, bf16[8,128,1024]{2,1,0:T(8,128)(2,1)}, u32[]{:S(2)}) %copy-start.3) | copy-done | bytes 2097176
  122.6 0.0 copy-start.4
  122.6 1.0 copy-done.4
  123.6 0.0 copy-start.5
  123.6 1.0 copy-done.5
  124.7 0.0 copy-start.6
  124.7 1.0 copy-done.6
  125.7 0.0 copy-start.9
  125.7 0.9 copy-done.9
  126.7 0.0 copy-start.10
  126.7 0.9 copy-done.10
  127.6 0.0 copy-start.11
  127.6 0.9 copy-done.11
  128.6 0.0 copy-start.13
  128.6 0.9 copy-done.13
  129.5 0.0 copy-start.14
  129.5 0.8 copy-done.14
  130.3 0.0 copy-start.15
  130.3 0.8 copy-done.15
  131.1 6.0 %shard_map.206 = (bf16[512,2048]{1,0:T(8,128)(2,1)}, bf16[512,2048]{1,0:T(8,128)(2,1)}, bf16[512,2048]{1,0:T(8,128)(2,1)}, f32[256,1024]{1,0:T(8,128)}, bf16[128...) custom-call(bf16[512,2048]{1,0:T(8,128)(2,1)S(1)} %copy-done, ...), custom_call_target="tpu_custom_call" | custom-call | flops 1000000000 | bytes 20000000 | tf_op jit(solution)/shard_map/pallas_call | solution.py:720
  137.1 0.7 copy.27
Async XLA Ops:
  4.9 111.3 %copy-start.7 = (f32[128,16]{1,0:T(8,128)S(1)}, f32[128,16]{1,0:T(8,128)}, u32[]{:S(2)}) copy-start(f32[128,16]{1,0:T(8,128)} %copy.23.steps_ref) | copy-start | bytes 24580
  4.9 111.3 %copy-start.8 = (bf16[128,1024]{1,0:T(8,128)(2,1)S(1)}, bf16[128,1024]{1,0:T(8,128)(2,1)}, u32[]{:S(2)}) copy-start(bf16[128,1024]{1,0:T(8,128)(2,1)} %v_ref.3) | copy-start | bytes 786436
  4.9 111.3 %copy-start.12 = (bf16[128,512]{1,0:T(8,128)(2,1)S(1)}, bf16[128,512]{1,0:T(8,128)(2,1)}, u32[]{:S(2)}) copy-start(bf16[128,512]{1,0:T(8,128)(2,1)} %b_ref.3) | copy-start | bytes 393220
  4.9 111.3 %copy-start.16 = (f32[16]{0:T(128)S(1)}, f32[16]{0:T(128)}, u32[]{:S(2)}) copy-start(f32[16]{0:T(128)} %param.19) | copy-start | bytes 196
  116.2 1.6 %copy-start = (bf16[512,2048]{1,0:T(8,128)(2,1)S(1)}, bf16[512,2048]{1,0:T(8,128)(2,1)}, u32[]{:S(2)}) copy-start(bf16[512,2048]{1,0:T(8,128)(2,1)} %get-tuple-element.31.dg_in) | copy-start | bytes 6291460
  117.8 1.6 %copy-start.1 = (bf16[512,2048]{1,0:T(8,128)(2,1)S(1)}, bf16[512,2048]{1,0:T(8,128)(2,1)}, u32[]{:S(2)}) copy-start(bf16[512,2048]{1,0:T(8,128)(2,1)} %get-tuple-element.32.du_in) | copy-start | bytes 6291460
  119.4 1.6 %copy-start.2 = (bf16[512,2048]{1,0:T(8,128)(2,1)S(1)}, bf16[512,2048]{1,0:T(8,128)(2,1)}, u32[]{:S(2)}) copy-start(bf16[512,2048]{1,0:T(8,128)(2,1)} %get-tuple-element.33.dd_in) | copy-start | bytes 6291460
  121.0 1.6 %copy-start.3 = (bf16[8,128,1024]{2,1,0:T(8,128)(2,1)S(1)}, bf16[8,128,1024]{2,1,0:T(8,128)(2,1)}, u32[]{:S(2)}) copy-start(bf16[8,128,1024]{2,1,0:T(8,128)(2,1)} %get-tuple-element.43.all_gated) | copy-start | bytes 6291460
  122.6 1.0 copy-start.4
  123.6 1.0 copy-start.5
  124.7 1.0 copy-start.6
  125.7 0.9 copy-start.9
  126.7 0.9 copy-start.10
  127.6 0.9 copy-start.11
  128.6 0.9 copy-start.13
  129.5 0.8 copy-start.14
  130.3 0.8 copy-start.15

commit v2 on v1

v2 whole, which is shorter than its diff:
```python
import functools

import jax
import jax.numpy as jnp
from jax import lax
from jax.experimental import pallas as pl
from jax.experimental.pallas import tpu as pltpu
from jax.sharding import PartitionSpec as P

NSTATE = 128
CLAMP_LIMIT = 7.0
SIGMOID_SCALE = 1.702
HIGHEST = lax.Precision.HIGHEST
F32 = jnp.float32
BF16 = jnp.bfloat16
NN = (((1,), (0,)), ((), ()))
NT = (((1,), (1,)), ((), ()))
TN = (((0,), (0,)), ((), ()))
MESH = pl.DeviceIdType.MESH


def mm(a, b, dims=NN):
    return lax.dot_general(a, b, dims, preferred_element_type=F32)


def mm_exact(a, b, dims=NN):
    return lax.dot_general(a, b, dims, precision=HIGHEST, preferred_element_type=F32)


def grid_of(rows, cols):
    return (
        lax.broadcasted_iota(jnp.int32, (rows, cols), 0),
        lax.broadcasted_iota(jnp.int32, (rows, cols), 1),
    )


def spread(heads, size):
    at, col = grid_of(heads, heads * size)
    return ((col >= at * size) & (col < (at + 1) * size)).astype(F32)


def fold(heads, size):
    col, at = grid_of(heads * size, heads)
    return ((col >= at * size) & (col < (at + 1) * size)).astype(F32)


def out(shape, dtype):
    return jax.ShapeDtypeStruct(shape, dtype)


def mixing_of(log_ref, logt_ref, h):
    length = log_ref.shape[0]
    row, col = grid_of(length, length)
    gap = log_ref[:, h : h + 1] - logt_ref[h : h + 1, :]
    return jnp.where(row >= col, jnp.exp(jnp.minimum(gap, 0.0)), 0.0)


def local_part(groups, v_ref, b_ref, c_ref, steps_ref, log_ref, logt_ref, y_ref, state_ref):
    heads = steps_ref.shape[1]
    per, size = heads // groups, v_ref.shape[1] // heads
    wide = per * size
    length = v_ref.shape[0]
    expand = spread(heads, size)
    to_end = jnp.exp(log_ref[length - 1 :, :] - log_ref[...])
    x = v_ref[...].astype(F32) * mm_exact(steps_ref[...], expand)
    xe = (x * mm_exact(to_end, expand)).astype(BF16)
    x = x.astype(BF16)
    for g in range(groups):
        keys = b_ref[:, g * NSTATE : (g + 1) * NSTATE]
        scores = mm(c_ref[:, g * NSTATE : (g + 1) * NSTATE], keys, NT)
        parts = []
        for r in range(per):
            h = g * per + r
            att = (scores * mixing_of(log_ref, logt_ref, h)).astype(BF16)
            parts.append(mm(att, x[:, h * size : (h + 1) * size]))
        y_ref[:, g * wide : (g + 1) * wide] = jnp.concatenate(parts, axis=1)
        state_ref[g * wide : (g + 1) * wide, :] = mm(
            xe[:, g * wide : (g + 1) * wide], keys, TN
        ).astype(BF16)


def enter_part(groups, y_ref, gate_ref, c_ref, log_ref, state_ref, out_ref, gated_ref):
    heads = log_ref.shape[1]
    per, size = heads // groups, y_ref.shape[1] // heads
    wide = per * size
    decay = mm_exact(jnp.exp(log_ref[...]), spread(heads, size))
    for g in range(groups):
        at = slice(g * wide, (g + 1) * wide)
        entered = mm(c_ref[:, g * NSTATE : (g + 1) * NSTATE], state_ref[at, :], NT) * decay[:, at]
        mixed = y_ref[:, at] + entered
        out_ref[:, at] = mixed
        gate = gate_ref[:, at].astype(F32)
        gated_ref[:, at] = (mixed * gate * jax.nn.sigmoid(gate)).astype(BF16)


def gate_part(groups, grad_ref, out_ref, gate_ref, c_ref, log_ref, gate_grad_ref, mixer_ref, state_ref):
    heads = log_ref.shape[1]
    wide = grad_ref.shape[1] // groups
    decay = mm_exact(jnp.exp(log_ref[...]), spread(heads, grad_ref.shape[1] // heads))
    for g in range(groups):
        at = slice(g * wide, (g + 1) * wide)
        gate = gate_ref[:, at].astype(F32)
        sig = jax.nn.sigmoid(gate)
        grad = grad_ref[:, at]
        gate_grad_ref[:, at] = (grad * out_ref[:, at] * sig * (1.0 + gate * (1.0 - sig))).astype(BF16)
        mixer = grad * gate * sig
        mixer_ref[:, at] = mixer
        keys = c_ref[:, g * NSTATE : (g + 1) * NSTATE]
        state_ref[at, :] = mm((mixer * decay[:, at]).astype(BF16), keys, TN).astype(BF16)


def inner_part(
    groups, v_ref, b_ref, c_ref, steps_ref, log_ref, logt_ref, mixer_ref, state_ref,
    out_keys_ref, in_part_ref, x_part_ref, base_ref,
):
    heads = steps_ref.shape[1]
    per, size = heads // groups, v_ref.shape[1] // heads
    wide = per * size
    length = v_ref.shape[0]
    row, col = grid_of(length, length)
    later = (row <= col).astype(BF16)
    expand = spread(heads, size)
    mixer = mixer_ref[...]
    decayed = mixer * mm_exact(jnp.exp(log_ref[...]), expand)
    decayed_low = decayed.astype(BF16)
    mixer = mixer.astype(BF16)
    x = (v_ref[...].astype(F32) * mm_exact(steps_ref[...], expand)).astype(BF16)
    entering = []
    _, head_at = grid_of(length, heads)
    pairs = jnp.zeros((length, heads), F32)
    for g in range(groups):
        at = slice(g * wide, (g + 1) * wide)
        keys_in = b_ref[:, g * NSTATE : (g + 1) * NSTATE]
        keys_out = c_ref[:, g * NSTATE : (g + 1) * NSTATE]
        scores = mm(keys_out, keys_in, NT)
        score_grad = jnp.zeros((length, length), F32)
        parts = []
        for r in range(per):
            h = g * per + r
            here = slice(h * size, (h + 1) * size)
            mixing = mixing_of(log_ref, logt_ref, h)
            att = scores * mixing
            att_grad = mm(mixer[:, here], x[:, here], NT)
            parts.append(mm(att.astype(BF16), mixer[:, here], TN))
            score_grad = score_grad + att_grad * mixing
            after = mm(later, (att_grad * att).astype(BF16))
            crossing = jnp.sum(jnp.where(col < row, after, 0.0), axis=1, keepdims=True)
            pairs = pairs + jnp.where(head_at == h, crossing, 0.0)
        x_part_ref[:, at] = jnp.concatenate(parts, axis=1)
        score_grad = score_grad.astype(BF16)
        state = state_ref[at, :]
        out_keys_ref[:, g * NSTATE : (g + 1) * NSTATE] = (
            mm(score_grad, keys_in) + mm(decayed_low[:, at], state)
        ).astype(BF16)
        in_part_ref[:, g * NSTATE : (g + 1) * NSTATE] = mm(score_grad, keys_out, TN)
        entering.append(decayed[:, at] * mm(keys_out, state, NT))
    entering = jnp.concatenate(entering, axis=1)
    sums = mm_exact(entering, fold(heads, size))
    base_ref[...] = pairs + mm_exact((row <= col).astype(F32), sums)


def outer_part(
    groups, after_ref, state_ref, v_ref, b_ref, steps_ref, log_ref, rates_ref,
    in_part_ref, x_part_ref, base_ref, values_ref, in_keys_ref, steps_grad_ref,
):
    heads = steps_ref.shape[1]
    per, size = heads // groups, v_ref.shape[1] // heads
    wide = per * size
    length = v_ref.shape[0]
    row, col = grid_of(length, length)
    expand = spread(heads, size)
    last = log_ref[length - 1 :, :]
    steps = mm_exact(steps_ref[...], expand)
    to_end = mm_exact(jnp.exp(last - log_ref[...]), expand)
    values = v_ref[...].astype(F32)
    xe = values * steps * to_end
    xe_low = xe.astype(BF16)
    leaving, direct = [], []
    _, head_at = grid_of(1, heads)
    passing = jnp.zeros((1, heads), F32)
    for g in range(groups):
        at = slice(g * wide, (g + 1) * wide)
        keys_in = b_ref[:, g * NSTATE : (g + 1) * NSTATE]
        for r in range(per):
            h = g * per + r
            here = slice(h * size, (h + 1) * size)
            both = after_ref[here, :] * state_ref[here, :].astype(F32)
            both = jnp.sum(jnp.sum(both, axis=0, keepdims=True), axis=1, keepdims=True)
            passing = passing + jnp.where(head_at == h, both, 0.0)
        after = after_ref[at, :].astype(BF16)
        reached = mm(keys_in, after, NT)
        x_grad = x_part_ref[:, at] + reached * to_end[:, at]
        values_ref[:, at] = (x_grad * steps[:, at]).astype(BF16)
        in_keys_ref[:, g * NSTATE : (g + 1) * NSTATE] = (
            in_part_ref[:, g * NSTATE : (g + 1) * NSTATE] + mm(xe_low[:, at], after)
        ).astype(BF16)
        leaving.append(reached * xe[:, at])
        direct.append(x_grad * values[:, at])
    gather = fold(heads, size)
    leaving = mm_exact(jnp.concatenate(leaving, axis=1), gather)
    direct = mm_exact(jnp.concatenate(direct, axis=1), gather)
    crossing = base_ref[...] + mm_exact((col < row).astype(F32), leaving) + jnp.exp(last) * passing
    steps_grad_ref[...] = (direct - rates_ref[...] * crossing).T


class Phase:
    def __init__(self):
        self.scope = None

    def __call__(self, name):
        if self.scope is not None:
            self.scope.__exit__(None, None, None)
        self.scope = name and jax.named_scope(name)
        if self.scope is not None:
            self.scope.__enter__()


class Sends:
    def __init__(self, sems):
        self.sems, self.used, self.open = sems, 0, []

    def block(self, count):
        self.used += count
        return self.used - count

    def copy(self, src, dst, landed, to, at):
        sem = self.sems.at[self.block(1) if at is None else at]
        return pltpu.make_async_remote_copy(
            src_ref=src, dst_ref=dst, send_sem=sem, recv_sem=landed,
            device_id=to, device_id_type=MESH,
        )

    def send(self, cond, src, dst, landed, to, at=None):
        copy = self.copy(src, dst, landed, to, at)
        when(cond, copy.start)
        self.open.append((cond, copy))

    def finish(self):
        assert self.used <= self.sems.shape[0]
        for cond, copy in self.open:
            when(cond, copy.wait_send)


def when(cond, action):
    if cond is None:
        action()
    else:
        pl.when(cond)(action)


def both(a, b):
    return a if b is None else b if a is None else a & b


class Place:
    def __init__(self, n, m):
        self.n, self.m, self.chips = n, m, n // 2
        self.s, self.t = lax.axis_index("sp"), lax.axis_index("tp")
        self.z, self.c = self.s // 2, lax.rem(self.s, 2)
        self.mate = self.z * 2 + 1 - self.c

    def around(self):
        for d in range(1, self.chips):
            for sign in (1, -1):
                at = self.z + sign * d
                yield d, at, (at >= 0) & (at < self.chips)

    def wait(self, cond, ref, sem):
        copy = pltpu.make_async_remote_copy(
            src_ref=ref, dst_ref=ref, send_sem=sem, recv_sem=sem,
            device_id=(self.mate, self.t), device_id_type=MESH,
        )
        when(cond, copy.wait_recv)

    def planes(self):
        for d in range(1, self.m):
            yield lax.rem(self.t + d, self.m)


class Line:
    def __init__(self, place, sends, own, block, landed):
        self.p, self.sends, self.own, self.block, self.landed = place, sends, own, block, landed

    def put(self, cond, src, owner, to):
        self.sends.send(cond, src, self.block(owner), self.landed.at[owner], (to, self.p.t))

    def begin(self, middle=None):
        p = self.p
        down, up = p.z > 0, p.z < p.chips - 1
        down_middle, up_middle = p.z == p.chips // 2, p.z == p.chips // 2 - 1
        if middle is None:
            self.put(down, self.own, p.s, p.s - 2)
            self.put(up, self.own, p.s, p.s + 2)
        elif middle:
            self.put(down_middle, self.own, p.s, p.s - 2)
            self.put(up_middle, self.own, p.s, p.s + 2)
        else:
            self.put(down & ~down_middle, self.own, p.s, p.s - 2)
            self.put(up & ~up_middle, self.own, p.s, p.s + 2)
        if not middle:
            self.put(None, self.own, p.s, p.mate)

    def step(self, d):
        p = self.p
        below, above = p.s - 2 * d, p.s + 2 * d
        from_below, from_above = p.z >= d, p.z + d < p.chips
        p.wait(from_below, self.block(below), self.landed.at[below])
        if d < p.chips - 1:
            self.put(from_below & (p.z < p.chips - 1), self.block(below), below, p.s + 2)
        self.put(from_below, self.block(below), below, p.mate)
        p.wait(from_above, self.block(above), self.landed.at[above])
        if d < p.chips - 1:
            self.put(from_above & (p.z > 0), self.block(above), above, p.s - 2)
        self.put(from_above, self.block(above), above, p.mate)

    def end(self):
        for k in range(self.p.chips):
            owner = 2 * k + 1 - self.p.c
            self.p.wait(None, self.block(owner), self.landed.at[owner])


class Chain:
    def __init__(self, place, sends, first, own, mates, span, mate_span, carry, onward, landed, swapped):
        self.p, self.sends, self.first = place, sends, first
        self.own, self.mates, self.span, self.mate_span = own, mates, span, mate_span
        self.carry, self.onward, self.landed, self.swapped = carry, onward, landed, swapped
        self.starts = place.z == (0 if first == 0 else place.chips - 1)
        self.stops = place.z == (place.chips - 1 if first == 0 else 0)
        self.next = place.s + (2 if first == 0 else -2)
        self.at = sends.block(2)

    def exchange(self):
        p = self.p
        self.sends.send(None, self.own, self.mates, self.swapped, (p.mate, p.t))

    def step(self, heads, size, only=None):
        p, c = self.p, self.p.c
        half = heads // 2
        rows = half * size

        def zero():
            self.carry[...] = jnp.zeros(self.carry.shape, self.carry.dtype)

        when(both(self.starts, only), zero)
        self.p.wait(both(~self.starts, only), self.carry.at[c], self.landed.at[0])
        self.sends.send(
            both(~self.starts, only), self.carry.at[c], self.carry.at[c], self.landed.at[1], (p.mate, p.t), self.at
        )

        def advance():
            mine, other = jnp.exp(self.span[0:1, :]), jnp.exp(self.mate_span[0:1, :])
            near = c == self.first
            for r in range(half):
                at = pl.ds(pl.multiple_of(c * rows + r * size, size), size)
                low, high = slice(r, r + 1), slice(half + r, half + r + 1)
                w_mine = jnp.where(c == 0, mine[:, low], mine[:, high])
                w_other = jnp.where(c == 0, other[:, low], other[:, high])
                own, mate = self.own[at, :].astype(F32), self.mates[at, :].astype(F32)
                carried = self.carry[c, r * size : (r + 1) * size, :].astype(F32)
                a = jnp.where(near, w_mine, w_other) * carried + jnp.where(near, own, mate)
                b = jnp.where(near, w_other, w_mine) * a + jnp.where(near, mate, own)
                self.onward[r * size : (r + 1) * size, :] = b.astype(BF16)

        go = both(~self.stops, only)
        when(go, advance)
        self.sends.send(go, self.onward, self.carry.at[c], self.landed.at[0], (self.next, p.t), self.at + 1)

    def finish(self, heads, size, target):
        p = self.p
        half = heads // 2
        rows = half * size
        self.p.wait(~self.starts, self.carry.at[1 - p.c], self.landed.at[1])
        other = jnp.exp(self.mate_span[0:1, :])
        near = p.c == self.first
        for h in range(heads):
            at = slice(h * size, (h + 1) * size)
            inside = slice((h % half) * size, (h % half + 1) * size)
            carried = self.carry[h // half, inside, :].astype(F32)
            through = other[:, h : h + 1] * carried + self.mates[at, :].astype(F32)
            target[at, :] = jnp.where(near, carried, through).astype(target.dtype)


def first_kernel(out_ref):
    out_ref[...] = jnp.zeros(out_ref.shape, out_ref.dtype)


def comm_kernel(
    cfg,
    v_ref, gate_ref, b_ref, c_ref, steps_t_ref, rates_ref, proj_ref, x_ref, g_ref, routes_t_ref, weights_t_ref,
    first_ref, wg_hbm, wu_hbm, wd_hbm,
    dg_ref, du_ref, dd_ref, grad_gate_ref, out_keys_ref, in_part_ref, x_part_ref, base_ref, log_ref,
    state_in, after_ref, all_stream, all_gated, steps_ref,
    wg, wu, wd, logt_ref, y_ref, mixer_out, gated, own_state, mate_state, own_grad, mate_grad,
    span, mate_span, carry_f, onward_f, carry_b, onward_b, gated_grad, mixer_grad,
    picked_ref, parts, local, rows, act, gate_g, up_g, back, shares, hop, reduced, returned, stream, full_proj,
    send_sems, load_sems, dz_in, dp_in, dq_in, hop_in, rs_in, rt_in, st_in, as_in, ag_in,
    low_in, high_in, gated_in, fwd_in, bwd_in, swap_in,
):
    n, m, groups, capp, width, share = cfg
    p = Place(n, m)
    wait = p.wait
    sends = Sends(send_sems)
    phase = Phase()
    top, tokens = routes_t_ref.shape
    heads = steps_t_ref.shape[0]
    size = v_ref.shape[1] // heads
    slots = n * capp
    model = x_ref.shape[1]
    hidden = wg.shape[0]
    quad = m == 4
    by_x, by_y, across = p.t + 1 - 2 * lax.rem(p.t, 2), lax.rem(p.t + 2, 4), 3 - p.t

    def cols(t):
        return pl.ds(pl.multiple_of(t * width, 128), width)

    mine = cols(p.t)

    phase("barrier")
    pairs = ((wg_hbm, wg), (wu_hbm, wu), (wd_hbm, wd))
    loads = [pltpu.make_async_copy(src, dst, load_sems.at[k]) for k, (src, dst) in enumerate(pairs)]
    for load in loads:
        load.start()
    barrier = pltpu.get_barrier_semaphore()
    for d in range(1, n):
        pl.semaphore_signal(barrier, inc=1, device_id=(lax.rem(p.s + d, n), p.t), device_id_type=MESH)
    for other in p.planes():
        pl.semaphore_signal(barrier, inc=1, device_id=(p.s, other), device_id_type=MESH)
    half_rows = proj_ref.shape[0] // 2
    low, high = pl.ds(0, half_rows), pl.ds(half_rows, half_rows)
    line_a = Line(p, sends, proj_ref.at[low], lambda s: full_proj.at[s, low], low_in)
    line_b = Line(p, sends, proj_ref.at[high], lambda s: full_proj.at[s, high], high_in)

    phase("slots")
    routes = routes_t_ref[...].T
    weights = weights_t_ref[...].T
    row, col = grid_of(tokens, tokens)
    _, expert = grid_of(tokens, n)
    _, slot = grid_of(tokens, slots)
    _, near = grid_of(tokens, 2 * capp)
    near = jnp.where(near < capp, p.s * capp + near, p.mate * capp + near - capp)
    hits = [expert == routes[:, k : k + 1] for k in range(top)]
    named = sum(hit.astype(F32) for hit in hits)
    before = mm((row > col).astype(BF16), named.astype(BF16))
    every = jnp.zeros((tokens, slots), F32)
    every_near = jnp.zeros((tokens, 2 * capp), F32)
    grads = jnp.zeros((slots, width), F32)
    g_part = g_ref[:, mine].astype(F32)
    nears = []
    for k in range(top):
        rank = jnp.sum(jnp.where(hits[k], before, 0.0), axis=1, keepdims=True).astype(jnp.int32)
        at = routes[:, k : k + 1] * capp + rank
        chosen = (slot == at).astype(F32)
        chosen_near = (near == at).astype(F32)
        every, every_near = every + chosen, every_near + chosen_near
        weight = weights[:, k : k + 1]
        grads = grads + mm(chosen.astype(BF16), (g_part * weight).astype(BF16), TN)
        nears.append((chosen_near.astype(BF16), weight))
    picked = every.astype(BF16)
    parts[0] = mm(picked, x_ref[:, mine], TN).astype(BF16).reshape(n, capp, width)
    parts[1] = grads.astype(BF16).reshape(n, capp, width)
    phase("dispatch")
    pl.semaphore_wait(barrier, n + m - 2)
    base = sends.block(n)
    for _, at, ok in p.around():
        for core in range(2):
            to = at * 2 + core
            sends.send(ok, parts.at[:, to], rows.at[:, p.s, :, mine], dz_in.at[p.s], (to, p.t), base + to)
    phase("near")
    picked_ref[...] = picked
    x_near = mm(every_near.astype(BF16), x_ref[...], TN).astype(BF16)
    grads_near = sum(
        mm(chosen, (g_ref[...].astype(F32) * weight).astype(BF16), TN) for chosen, weight in nears
    ).astype(BF16)
    local[0] = x_near[capp:]
    local[1] = grads_near[capp:]
    sends.send(None, local, rows.at[:, p.s], dz_in.at[p.s], (p.mate, p.t))
    rows[0, p.s] = x_near[:capp]
    rows[1, p.s] = grads_near[:capp]

    phase("local")
    steps_ref[...] = steps_t_ref[...].T
    log = mm_exact((row >= col).astype(F32), -steps_ref[...] * rates_ref[...])
    log_ref[...] = log
    logt_ref[...] = log.T
    span[...] = jnp.zeros(span.shape, F32)
    span[0:1, 0:heads] = log[tokens - 1 :, :]
    local_part(groups, v_ref, b_ref, c_ref, steps_ref, log_ref, logt_ref, y_ref, own_state)
    forward = Chain(
        p, sends, 0, own_state, mate_state, span, mate_span, carry_f, onward_f, fwd_in, swap_in.at[0]
    )
    forward.exchange()
    sends.send(None, span, mate_span, swap_in.at[2], (p.mate, p.t))

    def pair_of(at, t):
        return rows.at[:, pl.ds(2 * at, 2), :, cols(t)]

    relay_base, turn_base = sends.block(p.chips * m), sends.block(p.chips * 2)

    def relay(d, only=None):
        phase(f"relay{d}")
        for sign in (1, -1):
            at = p.z + sign * d
            ok = both((at >= 0) & (at < p.chips), only)
            for core in range(2):
                source = at * 2 + core
                wait(ok, rows.at[:, source, :, mine], dz_in.at[source])
            block = pair_of(at, p.t)
            for other in (by_x, by_y) if quad else p.planes():
                sends.send(ok, block, block, dp_in.at[at, p.t], (p.s, other), relay_base + at * m + other)

    def turn(d):
        if not quad:
            return
        phase(f"turn{d}")
        for sign in (1, -1):
            at = p.z + sign * d
            ok = (at >= 0) & (at < p.chips)
            for k, (source, to) in enumerate(((by_x, by_y), (by_y, by_x))):
                wait(ok, pair_of(at, source), dp_in.at[at, source])
                block = rows.at[k, pl.ds(2 * at, 2), :, cols(source)]
                sends.send(ok, block, block, dq_in.at[at, k], (p.s, to), turn_base + at * 2 + k)

    side = p.chips // 2

    def landed(ok, at):
        ok = ok & (at != p.z)
        if quad:
            for k in range(2):
                wait(ok, rows.at[k, pl.ds(2 * at, 2), :, cols(across)], dq_in.at[at, k])
        else:
            for other in p.planes():
                wait(ok, pair_of(at, other), dp_in.at[at, other])

    chunk = min(256, hidden)
    half = slots // 2
    flip = p.z // side
    sides = (flip, 1 - flip)
    pair = 2 * capp

    def in_side(side_at):
        return [(side_at * side + k) for k in range(side)]

    def experts_of(side_at):
        sources = pl.ds(side_at * (n // 2), n // 2)
        here = pl.ds(pl.multiple_of(side_at * half, half), half)

        def experts(k, _):
            at = pl.ds(pl.multiple_of(k * chunk, chunk), chunk)
            in_rows = rows[0, sources].reshape(half, model)
            gate_pre = mm(in_rows, wg[at, :], NT)
            up_pre = mm(in_rows, wu[at, :], NT)
            act_grad = mm(rows[1, sources].reshape(half, model), wd[at, :], NT)
            gate_clamped = jnp.minimum(gate_pre, CLAMP_LIMIT)
            up_clamped = jnp.clip(up_pre, -CLAMP_LIMIT, CLAMP_LIMIT) + 1.0
            sig = jax.nn.sigmoid(SIGMOID_SCALE * gate_clamped)
            swish = gate_clamped * sig
            act[here, at] = (up_clamped * swish).astype(BF16)
            gate_g[here, at] = jnp.where(
                gate_pre < CLAMP_LIMIT,
                act_grad * up_clamped * sig * (1.0 + SIGMOID_SCALE * gate_clamped * (1.0 - sig)),
                0.0,
            ).astype(BF16)
            up_g[here, at] = jnp.where(jnp.abs(up_pre) < CLAMP_LIMIT, act_grad * swish, 0.0).astype(BF16)
            return 0

        lax.fori_loop(0, hidden // chunk, experts, 0)

        def backs(q, _):
            at = cols(q)
            back[q, here] = (mm(gate_g[here, :], wg[:, at]) + mm(up_g[here, :], wu[:, at])).astype(BF16)
            return 0

        lax.fori_loop(0, m, backs, 0)

    def span_of(at):
        return pl.ds(pl.multiple_of(at * pair, pair), pair)

    def halves_of(at):
        return [pl.ds(pl.multiple_of(at * pair + k * capp, capp), capp) for k in range(2)]

    def reduce_send(at):
        if quad:
            first, second = halves_of(at)
            sends.send(None, back.at[across, first], hop.at[at, 0], hop_in.at[at, 0], (p.s, by_x))
            sends.send(None, back.at[across, second], hop.at[at, 1], hop_in.at[at, 1], (p.s, by_y))
        else:
            here = span_of(at)
            for other in p.planes():
                sends.send(None, back.at[other, here], shares.at[p.t, here], rs_in.at[at, p.t], (p.s, other))

    def reduce_turn(at):
        if not quad:
            return
        here = span_of(at)
        for k, (to, part) in enumerate(zip((by_y, by_x), halves_of(at))):
            wait(None, hop.at[at, k], hop_in.at[at, k])
            back[to, part] = (back[to, part].astype(F32) + hop[at, k].astype(F32)).astype(BF16)
            sends.send(None, back.at[to, here], shares.at[1 - k, here], rs_in.at[at, 1 - k], (p.s, to))

    def reduce_end(at):
        here = span_of(at)
        total = back[p.t, here].astype(F32)
        for other in (0, 1) if quad else p.planes():
            wait(None, shares.at[other, here], rs_in.at[at, other])
            total = total + shares[other, here].astype(F32)
        reduced[pl.ds(2 * at, 2)] = total.astype(BF16).reshape(2, capp, width)
        for core in range(2):
            to = 2 * at + core
            sends.send(to != p.s, reduced.at[to], returned.at[p.s], rt_in.at[p.s], (to, p.t))

    relay(1)
    phase("chain0")
    wait(None, mate_state, swap_in.at[0])
    wait(None, mate_span, swap_in.at[2])
    forward.step(heads, size, only=p.z == 0)
    line_a.begin(middle=False)
    full_proj[p.s] = proj_ref[...]
    middle = (p.z == side - 1) | (p.z == side)
    if p.chips > 2:
        relay(2, middle)
    turn(1)
    line_a.begin(middle=True)
    line_b.begin()

    phase("near_wait")
    for load in loads:
        load.wait()
    wait(None, rows.at[:, p.mate], dz_in.at[p.mate])
    for at in in_side(sides[0]):
        landed(at >= 0, at)
    phase("near_experts")
    experts_of(sides[0])
    for at in in_side(sides[0]):
        reduce_send(at)
    if p.chips > 2:
        relay(2, ~middle)
    for d in range(3, p.chips):
        relay(d)
    for d in range(2, p.chips):
        turn(d)
    phase("line_a1")
    line_a.step(1)
    if p.chips > 2:
        phase("chain1")
        forward.step(heads, size, only=p.z == 1)
    phase("far_wait")
    for at in in_side(sides[1]):
        landed(at >= 0, at)
    phase("near_turn")
    for at in in_side(sides[0]):
        reduce_turn(at)
    phase("far_experts")
    experts_of(sides[1])
    for at in in_side(sides[1]):
        reduce_send(at)
    phase("line_b1")
    line_b.step(1)
    phase("near_reduce")
    for at in in_side(sides[0]):
        reduce_end(at)

    def weight_grads(k, _):
        at = pl.ds(pl.multiple_of(k * chunk, chunk), chunk)
        in_rows = rows[0].reshape(slots, model)
        dg_ref[at, :] = mm(gate_g[:, at], in_rows, TN).astype(BF16)
        du_ref[at, :] = mm(up_g[:, at], in_rows, TN).astype(BF16)
        dd_ref[at, :] = mm(act[:, at], rows[1].reshape(slots, model), TN).astype(BF16)
        return 0

    phase("wgrads0")
    loops = hidden // chunk
    lax.fori_loop(0, (loops + 1) // 2, weight_grads, 0)
    phase("far_turn")
    for at in in_side(sides[1]):
        reduce_turn(at)
    phase("chain2")
    for d in range(2, p.chips - 1):
        forward.step(heads, size, only=p.z == d)
    phase("line_a2")
    if p.chips > 2:
        line_a.step(2)
    phase("wgrads1")
    if loops > 1:
        lax.fori_loop((loops + 1) // 2, loops, weight_grads, 0)
    phase("far_reduce")
    for at in in_side(sides[1]):
        reduce_end(at)
    returned[p.s] = reduced[p.s]
    phase("line_b2")
    if p.chips > 2:
        line_b.step(2)
    phase("chain3")
    forward.step(heads, size, only=p.z == p.chips - 1)
    forward.finish(heads, size, state_in)
    phase("enter")
    enter_part(groups, y_ref, gate_ref, c_ref, log_ref, state_in, mixer_out, gated)
    all_gated[p.s] = gated[...]
    gather = Line(p, sends, gated, lambda s: all_gated.at[s], gated_in)
    gather.begin()
    phase("line_3")
    for d in range(3, p.chips):
        line_a.step(d)
        line_b.step(d)
    phase("ret_wait")
    for d in range(1, n):
        source = lax.rem(p.s + d, n)
        wait(None, returned.at[source], rt_in.at[source])
    phase("combine")
    stream[:, mine] = (g_ref[:, mine].astype(F32) + mm(picked_ref[...], returned[...].reshape(slots, width))).astype(BF16)
    for other in p.planes():
        sends.send(None, stream.at[:, mine], stream.at[:, mine], st_in.at[p.t], (p.s, other))
    phase("st_wait")
    for other in p.planes():
        wait(None, stream.at[:, cols(other)], st_in.at[other])
    step = max(share, 128)
    part = tokens // m
    split = part % 16 == 0
    some = pl.ds(pl.multiple_of(p.t * part, part), part) if split else pl.ds(0, tokens)

    def columns(j):
        return pl.ds(pl.multiple_of(j * share // step * step, 128), step)

    base = sends.block(n)
    for _, at, ok in p.around():
        for core in range(2):
            to = at * 2 + core
            sends.send(
                ok, stream.at[some, columns(to)], all_stream.at[p.s, some], as_in.at[p.s], (to, p.t), base + to
            )
    sends.send(None, stream.at[some, columns(p.mate)], all_stream.at[p.s, some], as_in.at[p.s], (p.mate, p.t))
    all_stream[p.s, some] = stream[some, columns(p.s)]
    phase("line_end")
    line_a.end()
    line_b.end()
    phase("gated_grad")
    gated_grad[...] = mm(stream[...], full_proj[...].reshape(model, v_ref.shape[1]))
    gate_part(groups, gated_grad, mixer_out, gate_ref, c_ref, log_ref, grad_gate_ref, mixer_grad, own_grad)
    phase("swap_b")
    backward = Chain(
        p, sends, 1, own_grad, mate_grad, span, mate_span, carry_b, onward_b, bwd_in, swap_in.at[1]
    )
    backward.exchange()
    gather.step(1)
    wait(None, mate_grad, swap_in.at[1])
    backward.step(heads, size, only=p.z == p.chips - 1)
    phase("inner")
    inner_part(
        groups, v_ref, b_ref, c_ref, steps_ref, log_ref, logt_ref, mixer_grad, state_in,
        out_keys_ref, in_part_ref, x_part_ref, base_ref,
    )
    phase("back1")
    backward.step(heads, size, only=p.z == p.chips - 2)
    phase("as_wait")
    for d in range(1, n):
        source = lax.rem(p.s + d, n)
        wait(None, all_stream.at[source, some], as_in.at[source])
    if split:
        for other in p.planes():
            sends.send(None, all_stream.at[:, some], all_stream.at[:, some], ag_in.at[p.t], (p.s, other))
    for d in range(2, p.chips):
        phase(f"gather{d}")
        gather.step(d)
        phase(f"back{d}")
        backward.step(heads, size, only=p.z == p.chips - 1 - d)
    phase("back_fin")
    backward.finish(heads, size, after_ref)
    phase("gather_end")
    gather.end()
    phase("ag_wait")
    if split:
        for other in p.planes():
            theirs = pl.ds(pl.multiple_of(other * part, part), part)
            wait(None, all_stream.at[:, theirs], ag_in.at[other])
    phase("fin")
    sends.finish()
    phase(None)


def last_kernel(
    cfg,
    dg_in, du_in, dd_in, grad_gate_in, out_keys_in, in_part_ref, x_part_ref, base_ref, log_ref,
    state_in, after_ref, all_stream, all_gated, steps_ref, v_ref, b_ref, rates_ref,
    dg_out, du_out, dd_out, proj_grad_ref, values_ref, grad_gate_ref, in_keys_ref, out_keys_ref, steps_grad_ref,
    sums, sems,
):
    n, m, groups, capp, width, share = cfg
    phase = Phase()
    phase("proj")
    outs = [
        pltpu.make_async_copy(src, dst, sems.at[k])
        for k, (src, dst) in enumerate(((dg_in, dg_out), (du_in, du_out), (dd_in, dd_out)))
    ]
    for copy in outs:
        copy.start()
    tokens = all_stream.shape[0] * all_stream.shape[1]
    step = all_stream.shape[2]
    grad = mm(all_stream[...].reshape(tokens, step), all_gated[...].reshape(tokens, all_gated.shape[2]), TN)
    if step == share:
        proj_grad_ref[...] = grad
    else:
        sums[...] = grad
        off = pl.multiple_of(lax.rem(lax.axis_index("sp"), step // share) * share, share)
        proj_grad_ref[...] = sums[pl.ds(off, share), :]
    phase("pass")
    grad_gate_ref[...] = grad_gate_in[...]
    out_keys_ref[...] = out_keys_in[...]
    phase("outer")
    outer_part(
        groups, after_ref, state_in, v_ref, b_ref, steps_ref, log_ref, rates_ref,
        in_part_ref, x_part_ref, base_ref, values_ref, in_keys_ref, steps_grad_ref,
    )
    phase("stores")
    for copy in outs:
        copy.wait()
    phase(None)


def body(
    mix_values, mix_gate, input_keys, output_keys, step_sizes, decay_rates, out_proj, expert_inputs,
    stream_grad, routes, route_weights, gate_proj, up_proj, down_proj,
):
    tokens, inner = mix_values.shape
    model = stream_grad.shape[1]
    top = routes.shape[1]
    n, m = lax.axis_size("sp"), lax.axis_size("tp")
    experts = gate_proj.shape[0] * n
    cap = 3 * tokens * top // (2 * experts)
    capp = -(-cap // 16) * 16
    slots = n * capp
    heads = step_sizes.shape[1]
    groups = input_keys.shape[1] // NSTATE
    width = model // m
    hidden = gate_proj.shape[1]
    share = model // n
    chips = n // 2
    step = max(share, 128)
    rates = decay_rates.reshape(1, heads)
    cfg = (n, m, groups, capp, width, share)
    vm, anyw = pl.BlockSpec(memory_space=pltpu.VMEM), pl.BlockSpec(memory_space=pl.ANY)
    keys_shape = input_keys.shape
    weight = (hidden, model)
    dma = pltpu.SemaphoreType.DMA
    sent = (
        2 * n + 6 + 4 + chips * (m + 2) + 2 * (5 + 4 * (chips - 1)) + 3 + 4 * (chips - 1)
        + chips * max(4, m - 1) + 2 * chips + 2 * (m - 1)
    )
    small = (
        mix_values, mix_gate, input_keys, output_keys, step_sizes.T, rates, out_proj, expert_inputs,
        stream_grad, routes.T, route_weights.T,
    )
    first = pl.pallas_call(
        first_kernel,
        out_shape=out((8, 128), F32),
        out_specs=vm,
        cost_estimate=pl.CostEstimate(flops=10**10, bytes_accessed=4096, transcendentals=0),
        compiler_params=pltpu.CompilerParams(vmem_limit_bytes=2**20),
    )()
    mids = pl.pallas_call(
        functools.partial(comm_kernel, cfg),
        out_shape=[
            out(weight, BF16), out(weight, BF16), out(weight, BF16),
            out((tokens, inner), BF16), out(keys_shape, BF16), out(keys_shape, F32),
            out((tokens, inner), F32), out((tokens, heads), F32), out((tokens, heads), F32),
            out((inner, NSTATE), BF16), out((inner, NSTATE), F32),
            out((n, tokens, step), BF16), out((n, tokens, inner), BF16), out((tokens, heads), F32),
        ],
        in_specs=[vm] * 11 + [anyw] * 4,
        out_specs=[vm] * 14,
        scratch_shapes=[
            pltpu.VMEM(weight, BF16), pltpu.VMEM(weight, BF16), pltpu.VMEM(weight, BF16),
            pltpu.VMEM((heads, tokens), F32),
            pltpu.VMEM((tokens, inner), F32), pltpu.VMEM((tokens, inner), F32), pltpu.VMEM((tokens, inner), BF16),
            pltpu.VMEM((inner, NSTATE), BF16), pltpu.VMEM((inner, NSTATE), BF16),
            pltpu.VMEM((inner, NSTATE), BF16), pltpu.VMEM((inner, NSTATE), BF16),
            pltpu.VMEM((8, 128), F32), pltpu.VMEM((8, 128), F32),
            pltpu.VMEM((2, inner // 2, NSTATE), BF16), pltpu.VMEM((inner // 2, NSTATE), BF16),
            pltpu.VMEM((2, inner // 2, NSTATE), BF16), pltpu.VMEM((inner // 2, NSTATE), BF16),
            pltpu.VMEM((tokens, inner), F32), pltpu.VMEM((tokens, inner), F32),
            pltpu.VMEM((tokens, slots), BF16),
            pltpu.VMEM((2, n, capp, width), BF16),
            pltpu.VMEM((2, capp, model), BF16),
            pltpu.VMEM((2, n, capp, model), BF16),
            pltpu.VMEM((slots, hidden), BF16), pltpu.VMEM((slots, hidden), BF16), pltpu.VMEM((slots, hidden), BF16),
            pltpu.VMEM((m, slots, width), BF16), pltpu.VMEM((2 if m == 4 else m, slots, width), BF16),
            pltpu.VMEM((chips, 2, capp, width), BF16),
            pltpu.VMEM((n, capp, width), BF16), pltpu.VMEM((n, capp, width), BF16),
            pltpu.VMEM((tokens, model), BF16),
            pltpu.VMEM((n,) + out_proj.shape, BF16),
            dma((sent,)), dma((3,)), dma((n,)), dma((chips, m)), dma((chips, 2)), dma((chips, 2)), dma((chips, m)),
            dma((n,)), dma((m,)), dma((n,)), dma((m,)),
            dma((n,)), dma((n,)), dma((n,)), dma((2,)), dma((2,)), dma((3,)),
        ],
        cost_estimate=pl.CostEstimate(flops=10**10, bytes_accessed=3 * 10**7, transcendentals=0),
        compiler_params=pltpu.CompilerParams(
            collective_id=0, has_side_effects=True, vmem_limit_bytes=40 * 2**20
        ),
    )(
        *small, first,
        gate_proj.reshape(weight), up_proj.reshape(weight), down_proj.reshape(weight),
    )
    log = mids[8]
    outs = pl.pallas_call(
        functools.partial(last_kernel, cfg),
        out_shape=[
            out(weight, BF16), out(weight, BF16), out(weight, BF16),
            out((share, inner), F32), out((tokens, inner), BF16), out((tokens, inner), BF16),
            out(keys_shape, BF16), out(keys_shape, BF16), out((heads, tokens), F32),
        ],
        in_specs=[vm] * 17,
        out_specs=[anyw] * 3 + [vm] * 6,
        scratch_shapes=[pltpu.VMEM((step, inner), F32), dma((3,))],
        cost_estimate=pl.CostEstimate(flops=10**9, bytes_accessed=2 * 10**7, transcendentals=0),
        compiler_params=pltpu.CompilerParams(vmem_limit_bytes=24 * 2**20),
    )(*mids, mix_values, input_keys, rates)
    shape = gate_proj.shape
    return tuple(o.reshape(shape) for o in outs[:3]) + tuple(outs[3:-1]) + (outs[-1].T,)


def solution(mesh):
    return jax.shard_map(
        body,
        mesh=mesh,
        in_specs=(
            P("sp", "tp"), P("sp", "tp"), P("sp", "tp"), P("sp", "tp"), P("sp", "tp"), P("tp"),
            P("sp", "tp"), P("sp", None), P("sp", None), P("sp", None), P("sp", None),
            P("sp", "tp", None), P("sp", "tp", None), P("sp", "tp", None),
        ),
        out_specs=(
            P("sp", "tp", None), P("sp", "tp", None), P("sp", "tp", None),
            P("sp", "tp"), P("sp", "tp"), P("sp", "tp"), P("sp", "tp"), P("sp", "tp"), P("sp", "tp"),
        ),
        check_vma=False,
    )
```

time: 139 us -> 102 us (0.73); the launches traced: 138 us -> 102 us
  local copies, waits for them, and re-layouts: 19.8 us -> 1.54 us
  Pallas kernels: 117 us -> 99.8 us
    unnamed x38 -> x22, local copies, waits for them, and re-layouts: 19.8 us -> 1.54 us
    pallas_call x1, Pallas kernels: 111 us -> 93 us  [body(): pl.pallas_call(functools.partial(comm_kernel, cfg), out_shape=[out(weight...]
where the time goes in v2:
time: 102 us
  Pallas kernels  99.8 us (98%)
  local copies, waits for them, and re-layouts  1.54 us (2%)
    pallas_call x1, Pallas kernels, body(): pl.pallas_call(functools.partial(comm_kernel, cfg), out_shape=[out(weight...  93 us
    pallas_call x1, Pallas kernels, body(): pl.pallas_call(functools.partial(last_kernel, cfg), out_shape=[out(weight...  6.8 us

profile of v2, /device:TPU:1, one launch (start us, length us, event | category | flops | bytes accessed | tf_op | source)
XLA Modules:
  0.0 102.2 jit_solution(2684145311604171390)
XLA Ops:
  0.6 0.0 copy-start
  0.7 0.0 copy-start.1
  0.7 0.0 copy-start.2
  0.7 0.0 copy-start.3
  0.7 0.0 copy-start.4
  0.7 0.0 copy-start.5
  0.7 0.0 copy-start.6
  0.7 0.0 copy-start.7
  0.7 0.0 copy-start.8
  0.7 0.0 copy-start.9
  0.7 0.0 copy-start.10
  0.8 0.8 copy-done
  1.6 0.0 copy-done.1
  1.6 0.0 copy-done.2
  1.6 0.2 copy-done.3
  1.9 0.2 copy-done.4
  2.0 0.2 copy-done.5
  2.2 0.1 copy-done.6
  2.2 0.0 copy-done.7
  2.3 0.0 copy-done.8
  2.3 0.0 copy-done.9
  2.3 0.0 copy-done.10
  2.3 93.0 %shard_map.206 = (bf16[512,2048]{1,0:T(8,128)(2,1)S(1)}, bf16[512,2048]{1,0:T(8,128)(2,1)S(1)}, bf16[512,2048]{1,0:T(8,128)(2,1)S(1)}, bf16[128,1024]{1,0:T(8,12...) custom-call(bf16[128,1024]{1,0:T(8,128)(2,1)S(1)} %copy-done, ...), custom_call_target="tpu_custom_call" | custom-call | flops 10000000000 | bytes 30000000 | tf_op jit(solution)/shard_map/pallas_call | solution.py:858
  95.3 6.8 %shard_map.207 = (bf16[512,2048]{1,0:T(8,128)(2,1)}, bf16[512,2048]{1,0:T(8,128)(2,1)}, bf16[512,2048]{1,0:T(8,128)(2,1)}, f32[256,1024]{1,0:T(8,128)}, bf16[128...) custom-call(bf16[512,2048]{1,0:T(8,128)(2,1)S(1)} %get-tuple-element, ...), custom_call_target="tpu_custom_call" | custom-call | flops 1000000000 | bytes 20000000 | tf_op jit(solution)/shard_map/pallas_call | solution.py:902
  (1 shorter events, 0.0 us)
Async XLA Ops:
  0.6 1.0 copy-start
  0.7 1.0 copy-start.1
  0.7 1.0 copy-start.2
  0.7 1.2 %copy-start.3 = (bf16[256,1024]{1,0:T(8,128)(2,1)S(1)}, bf16[256,1024]{1,0:T(8,128)(2,1)}, u32[]{:S(2)}) copy-start(bf16[256,1024]{1,0:T(8,128)(2,1)} %proj_ref.1) | copy-start | bytes 1572868
  0.7 1.3 %copy-start.4 = (bf16[128,2048]{1,0:T(8,128)(2,1)S(1)}, bf16[128,2048]{1,0:T(8,128)(2,1)}, u32[]{:S(2)}) copy-start(bf16[128,2048]{1,0:T(8,128)(2,1)} %x_ref.1) | copy-start | bytes 1572868
  0.7 1.5 %copy-start.5 = (bf16[128,2048]{1,0:T(8,128)(2,1)S(1)}, bf16[128,2048]{1,0:T(8,128)(2,1)}, u32[]{:S(2)}) copy-start(bf16[128,2048]{1,0:T(8,128)(2,1)} %g_ref.1) | copy-start | bytes 1572868
  0.7 1.5 %copy-start.6 = (bf16[128,1024]{1,0:T(8,128)(2,1)S(1)}, bf16[128,1024]{1,0:T(8,128)(2,1)}, u32[]{:S(2)}) copy-start(bf16[128,1024]{1,0:T(8,128)(2,1)} %gate_ref.1) | copy-start | bytes 786436
  0.7 1.6 %copy-start.7 = (bf16[128,512]{1,0:T(8,128)(2,1)S(1)}, bf16[128,512]{1,0:T(8,128)(2,1)}, u32[]{:S(2)}) copy-start(bf16[128,512]{1,0:T(8,128)(2,1)} %c_ref.1) | copy-start | bytes 393220
  0.7 1.6 %copy-start.8 = (f32[128,16]{0,1:T(8,128)S(1)}, f32[128,16]{0,1:T(8,128)}, u32[]{:S(2)}) copy-start(f32[128,16]{0,1:T(8,128)} %param.18) | copy-start | bytes 24580
  0.7 1.5 %copy-start.9 = (s32[128,2]{0,1:T(2,128)S(1)}, s32[128,2]{0,1:T(2,128)}, u32[]{:S(2)}) copy-start(s32[128,2]{0,1:T(2,128)} %param.23) | copy-start | bytes 3076
  0.7 1.5 %copy-start.10 = (f32[128,2]{0,1:T(2,128)S(1)}, f32[128,2]{0,1:T(2,128)}, u32[]{:S(2)}) copy-start(f32[128,2]{0,1:T(2,128)} %param.24) | copy-start | bytes 3076
